TPU v7x, 128 devices: a whole 4x4x4 slice. The times are simulated.
128 devices in a mesh: sp: 16 (over z, x), dp: 8 (over y, core).
Axes of the slice: x: 4, y: 4, z: 4, core: 2. Of those that a mesh axis runs over, the one named last changes fastest.
Arguments:
- residual_in: bfloat16 [8, 2048, 2048], P('dp', 'sp'), may hold values from -6 to 6
- query_proj: bfloat16 [8, 2048, 2048], P('dp', 'sp'), may hold values from -8 to 8
- key_proj: bfloat16 [8, 2048, 512], P('dp', 'sp'), may hold values from -8 to 8
- value_proj: bfloat16 [8, 2048, 512], P('dp', 'sp'), may hold values from -6 to 6
- query_gain: float32 [128], replicated, may hold values from 0.1 to 7
- key_gain: float32 [128], replicated, may hold values from 0.1 to 7
- out_weight: bfloat16 [2048, 2048], replicated, may hold values from -0.125 to 0.125
- post_gain: float32 [2048], replicated, may hold values from 0.1 to 1.9
- pre_gain: float32 [2048], replicated, may hold values from 0.1 to 1.9
- route_ids: int32 [8, 2048, 2], P('dp', 'sp'), may hold values from 0 to 127, as said below
- group_weight: float32 [8, 2048], P('dp', 'sp'), may hold values from 0.25 to 1
- first_share: float32 [8, 2048], P('dp', 'sp'), may hold values from 0.5 to 1
- gate_weight: bfloat16 [128, 2048, 512], P(('sp', 'dp')), may hold values from -0.125 to 0.125
- up_weight: bfloat16 [128, 2048, 512], P(('sp', 'dp')), may hold values from -0.125 to 0.125
- down_weight: bfloat16 [128, 512, 2048], P(('sp', 'dp')), may hold values from -0.25 to 0.25
Outputs:
- layer_out: bfloat16 [8, 2048, 2048], P('dp', 'sp')
Inputs may be any that keep to these rules, and one draw needn't show every extreme that they name: `route_ids`: each token names two different experts of one group of 32 consecutive experts. Among the 128 tokens of one device each group is chosen by exactly 32 tokens, no expert is named by more than 4 of them, and in every draw one expert of each group is named by exactly 4 tokens of every device.
All inputs are finite; a program needn't handle non-finite values.
Results may differ from a plain program's by a relative error of at most 0.009.
The roundings to bfloat16 on the way count: a program that leaves them out, or rounds other values in their place, can miss the bound.
Values may be sent and summed in bfloat16 or wider, within the bound.
No kernel may reach another device: no remote copies, remote signals or barrier semaphores. Data moves between devices by JAX's collectives and lax.ppermute only.
A program may use at most 128 MiB of HBM per device.

v0:
```python
import jax
import jax.numpy as jnp
from jax import lax
from jax.sharding import PartitionSpec as P

HEADS = 16
KV_HEADS = 4
HEAD_DIM = 128
GRID_W = 64


EPSILON = 1e-06


def side_by_side(arrays, axis, dim, along):
    ends, at = ([], 0)
    for a in arrays[:-1]:
        at += a.shape[along]
        ends.append(at)
    both = jnp.concatenate(arrays, axis=along)
    return tuple(jnp.split(lax.all_gather(both, axis, axis=dim, tiled=True), ends, axis=along))


def rotate_heads(raw_heads, gain_vec, positions):
    floats = raw_heads.astype(jnp.float32)
    normed = (
        floats * lax.rsqrt(jnp.mean(floats * floats, axis=-1, keepdims=True) + EPSILON) * gain_vec
    )
    quarter = raw_heads.shape[-1] // 4
    inverse = 10000.0 ** (-jnp.arange(quarter, dtype=jnp.float32) / quarter)
    grid_rows = (positions // GRID_W).astype(jnp.float32)[:, None] * inverse
    grid_cols = (positions % GRID_W).astype(jnp.float32)[:, None] * inverse
    angles = jnp.concatenate([grid_rows, grid_rows, grid_cols, grid_cols], axis=-1)[:, None, :]
    pieces = normed.reshape(normed.shape[:-1] + (2, 2, quarter))
    turned = jnp.stack([-pieces[..., 1, :], pieces[..., 0, :]], axis=-2).reshape(normed.shape)
    return (normed * jnp.cos(angles) + turned * jnp.sin(angles)).astype(jnp.bfloat16)


def attend_blocks(queries, keys_all, values_all):
    count_q, kv_count, group_size, head_width = queries.shape
    block = min(512, count_q)
    blocks = count_q // block
    scale = head_width ** (-0.5)
    zero_index = jnp.zeros((), jnp.int32)

    def one_item(item):
        which = item // kv_count
        head_index = item % kv_count
        start_row = which * block
        q_block = lax.dynamic_slice(
            queries,
            (start_row, head_index, zero_index, zero_index),
            (block, 1, group_size, head_width),
        )[:, 0]
        key_block = lax.dynamic_slice(
            keys_all, (zero_index, head_index, zero_index), (keys_all.shape[0], 1, head_width)
        )[:, 0]
        value_block = lax.dynamic_slice(
            values_all, (zero_index, head_index, zero_index), (values_all.shape[0], 1, head_width)
        )[:, 0]
        scores = (
            jnp.einsum("qgd,sd->gqs", q_block, key_block, preferred_element_type=jnp.float32)
            * scale
        )
        shifted = jnp.exp(scores - jnp.max(scores, axis=-1, keepdims=True))
        weights = (shifted / jnp.sum(shifted, axis=-1, keepdims=True)).astype(jnp.bfloat16)
        return jnp.einsum(
            "gqs,sd->qgd", weights, value_block, preferred_element_type=jnp.float32
        ).astype(jnp.bfloat16)

    results = lax.map(one_item, jnp.arange(blocks * kv_count, dtype=jnp.int32))
    results = results.reshape(blocks, kv_count, block, group_size, head_width).transpose(
        0, 2, 1, 3, 4
    )
    return results.reshape(count_q, kv_count * group_size * head_width)


def rms_scale(values, gain_vec):
    floats = values.astype(jnp.float32)
    return (
        floats * lax.rsqrt(jnp.mean(floats * floats, axis=-1, keepdims=True) + EPSILON) * gain_vec
    )


def expert_ffn(arrived, gate_weight, up_weight, down_weight):
    gated = jnp.einsum("nesd,edf->nesf", arrived, gate_weight, preferred_element_type=jnp.float32)
    lifted = jnp.einsum("nesd,edf->nesf", arrived, up_weight, preferred_element_type=jnp.float32)
    hidden = (jax.nn.silu(gated) * lifted).astype(jnp.bfloat16)
    return jnp.einsum(
        "nesf,efd->nesd", hidden, down_weight, preferred_element_type=jnp.float32
    ).astype(jnp.bfloat16)


def local(
    residual_in,
    query_proj,
    key_proj,
    value_proj,
    query_gain,
    key_gain,
    out_weight,
    post_gain,
    pre_gain,
    route_ids,
    group_weight,
    first_share,
    gate_weight,
    up_weight,
    down_weight,
):
    sp_count = lax.axis_size("sp")
    dp_count = lax.axis_size("dp")
    tokens = query_proj.shape[1]
    group_size = HEADS // KV_HEADS
    key_all, value_all = side_by_side((key_proj, value_proj), "sp", 1, 0)
    length = key_all.shape[1]
    key_positions = jnp.arange(length, dtype=jnp.int32)
    query_positions = lax.axis_index("sp") * tokens + jnp.arange(tokens, dtype=jnp.int32)
    query_turned = rotate_heads(
        query_proj.reshape(tokens, HEADS, HEAD_DIM), query_gain, query_positions
    )
    key_turned = rotate_heads(key_all.reshape(length, KV_HEADS, HEAD_DIM), key_gain, key_positions)
    attended = attend_blocks(
        query_turned.reshape(tokens, KV_HEADS, group_size, HEAD_DIM),
        key_turned,
        value_all.reshape(length, KV_HEADS, HEAD_DIM),
    )
    mixed = jnp.dot(attended, out_weight, preferred_element_type=jnp.float32).astype(jnp.bfloat16)
    stream = (residual_in[0].astype(jnp.float32) + rms_scale(mixed, post_gain)).astype(jnp.bfloat16)
    normed = rms_scale(stream, pre_gain).astype(jnp.bfloat16)
    model_width = normed.shape[1]
    local_experts = gate_weight.shape[0]
    expert_count = local_experts * sp_count * dp_count
    capacity = 4 * tokens // expert_count
    chosen = route_ids.reshape(2 * tokens)
    onehot = (chosen[:, None] == jnp.arange(expert_count, dtype=jnp.int32)[None, :]).astype(
        jnp.int32
    )
    earlier = jnp.cumsum(onehot, axis=0) - onehot
    slot_rank = jnp.sum(earlier * onehot, axis=1)
    slot_index = chosen * capacity + slot_rank
    source_row = (
        jnp.full((expert_count * capacity,), tokens, jnp.int32)
        .at[slot_index]
        .set(jnp.arange(2 * tokens, dtype=jnp.int32) // 2)
    )
    padded = jnp.concatenate([normed, jnp.zeros((1, model_width), jnp.bfloat16)], axis=0)
    outgoing = padded[source_row]
    shaped = outgoing.reshape(sp_count * dp_count, local_experts, capacity, model_width)
    answered = expert_ffn(
        lax.all_to_all(shaped, ("sp", "dp"), split_axis=0, concat_axis=0, tiled=True),
        gate_weight,
        up_weight,
        down_weight,
    )
    returned = lax.all_to_all(answered, ("sp", "dp"), split_axis=0, concat_axis=0, tiled=True)
    results = (
        returned.reshape(expert_count * capacity, model_width)[slot_index]
        .astype(jnp.float32)
        .reshape(tokens, 2, model_width)
    )
    share = first_share[0]
    weight_pair = group_weight[0][:, None] * jnp.stack([share, 1.0 - share], axis=1)
    combined = jnp.sum(weight_pair[:, :, None] * results, axis=1)
    return (
        (stream.astype(jnp.float32) + combined).astype(jnp.bfloat16).reshape(1, tokens, model_width)
    )


def solution(mesh):
    placed = (
        P("dp", "sp", None),
        P("dp", "sp", None),
        P("dp", "sp", None),
        P("dp", "sp", None),
        P(),
        P(),
        P(),
        P(),
        P(),
        P("dp", "sp", None),
        P("dp", "sp"),
        P("dp", "sp"),
        P(("sp", "dp"), None, None),
        P(("sp", "dp"), None, None),
        P(("sp", "dp"), None, None),
    )
    return jax.shard_map(
        local, mesh=mesh, in_specs=placed, out_specs=P("dp", "sp", None), check_vma=False
    )
```

profile of v0, /device:TPU:0, one launch (start us, length us, event | category | flops | bytes accessed | tf_op | source)
XLA Modules:
  0.0 257.9 jit_solution(9064251186789726735)
XLA Ops:
  6.5 1.2 copy.36
  7.7 1.0 copy.37
  8.8 0.7 pad_maximum_fusion.3
  9.5 0.8 copy.43
  10.6 0.7 mul.306
  11.3 2.1 copy.38
  13.4 1.1 convert_element_type.179
  16.0 2.1 convert_multiply_fusion.2
  18.0 1.3 reduce_sum.69
  19.5 1.6 scatter_custom_fusion
  22.0 4.6 %fusion.72 = (f32[2048,128]{0,1:T(8,128)}, f32[2048,128]{0,1:T(8,128)}) fusion(f32[2048,32]{0,1:T(8,128)S(1)} %get-tuple-element.123, f32[2048,32]{0,1:T(8,128)S(1)} %get-tuple-element.122), kind=kLoop, calls=%fused_computation.69 | loop fusion | flops 786432 | bytes 2621440 | tf_op jit(solution)/shard_map/cos | solution.py:36
  26.6 1.1 add_convert_fusion
  27.7 41.4 %all-gather.2.cloned.1.call-done = bf16[2,2048,512]{1,2,0:T(8,128)(2,1)} async-done(((bf16[2,128,512]{1,2,0:T(8,128)(2,1)}), bf16[2,2048,512]{1,2,0:T(8,128)(2,1)}) %all-gather.2.cloned.1.call-update) | async-done | bytes 4194320 | tf_op jit(solution)/shard_map/all_gather | solution.py:21
  69.1 4.3 %slice_convert_fusion = (f32[1,2048,512]{1,2,0:T(8,128)S(1)}, bf16[1,2048,512]{1,2,0:T(8,128)(2,1)}) fusion(bf16[2,2048,512]{1,2,0:T(8,128)(2,1)} %all-gather.2.cloned.1.call-done), kind=kLoop, calls=%fused_computation.38 | loop fusion | flops 1048576 | bytes 10485760 | tf_op jit(solution)/shard_map/convert_element_type | solution.py:25
  75.5 0.9 copy-done.2
  76.7 2.8 %fusion.29 = bf16[2048,4,128]{0,2,1:T(8,128)(2,1)} fusion(f32[2048,4,2,2,32]{0,4,3,2,1:T(8,128)S(1)} %pad_maximum_fusion, f32[2048,4,128]{0,2,1:T(8,128)S(1)} %bitcast.174, f32[2048,128]{0,1:T(8,128)S(1)} %copy-done.3, f32[2048,128]{0,1:T(8,128)S(1)} %copy-done.2, f32[128]{0:T(128)S(1)} %copy-done.11, f32[2048,4]{0,1:T(4,128)S(1)} %add_rsqrt_fusion), kind=kLoop, calls=%fused_computation.30 | loop fusion | flops 6291456 | bytes 12616192 | tf_op jit(solution)/shard_map/convert_element_type | solution.py:36
  79.5 49.5 %while.12 = (s32[]{:T(128)}, bf16[4,128,4,128]{1,3,2,0:T(8,128)(2,1)S(1)}, s32[4]{0:T(128)S(1)}, bf16[2048,4,128]{0,2,1:T(8,128)(2,1)}, bf16[2048,4,128]{0,2,1:T...) while((s32[]{:T(128)}, ...), condition=%wide.region_5.6_spmd, body=%wide.region_2.5_spmd.sunk | while | flops 546378240 | bytes 34871072 | solution.py:71
  82.1 1.8 fusion.115
  83.9 1.9 copy-done.1
  85.8 1.1 fusion.116
  86.9 5.0 %fusion.117 = bf16[4,128,4,128]{1,3,2,0:T(8,128)(2,1)S(1)} fusion(bf16[4,128,4,128]{1,3,2,0:T(8,128)(2,1)S(1)} %get-tuple-element.178, s32[]{:T(128)} %get-tuple-element.177, f32[4,128]{1,0:T(4,128)S(1)} %fusion.116, bf16[2048,4,128]{0,2,1:T(8,128)(2,1)} %get-tuple-element.190, s32[]{:T(128)S(6)} %select_n.109, f32[2048,128,4]{1,0,2:T(8,128)} %copy-done.1), kind=kOutput, calls=%fused_computation.14.clone.1 | convolution fusion | flops 273746432 | bytes 9046532 | tf_op jit(solution)/shard_map/while/body/eval_jaxpr/gqs,sd->qgd/dot_general | solution.py:67
  94.5 1.8 fusion.115
  96.3 1.9 copy-done.1
  98.2 1.1 fusion.116
  99.3 5.0 %fusion.117 = bf16[4,128,4,128]{1,3,2,0:T(8,128)(2,1)S(1)} fusion(bf16[4,128,4,128]{1,3,2,0:T(8,128)(2,1)S(1)} %get-tuple-element.178, s32[]{:T(128)} %get-tuple-element.177, f32[4,128]{1,0:T(4,128)S(1)} %fusion.116, bf16[2048,4,128]{0,2,1:T(8,128)(2,1)} %get-tuple-element.190, s32[]{:T(128)S(6)} %select_n.109, f32[2048,128,4]{1,0,2:T(8,128)} %copy-done.1), kind=kOutput, calls=%fused_computation.14.clone.1 | convolution fusion | flops 273746432 | bytes 9046532 | tf_op jit(solution)/shard_map/while/body/eval_jaxpr/gqs,sd->qgd/dot_general | solution.py:67
  106.9 1.8 fusion.115
  108.7 1.9 copy-done.1
  110.6 1.1 fusion.116
  111.7 5.0 %fusion.117 = bf16[4,128,4,128]{1,3,2,0:T(8,128)(2,1)S(1)} fusion(bf16[4,128,4,128]{1,3,2,0:T(8,128)(2,1)S(1)} %get-tuple-element.178, s32[]{:T(128)} %get-tuple-element.177, f32[4,128]{1,0:T(4,128)S(1)} %fusion.116, bf16[2048,4,128]{0,2,1:T(8,128)(2,1)} %get-tuple-element.190, s32[]{:T(128)S(6)} %select_n.109, f32[2048,128,4]{1,0,2:T(8,128)} %copy-done.1), kind=kOutput, calls=%fused_computation.14.clone.1 | convolution fusion | flops 273746432 | bytes 9046532 | tf_op jit(solution)/shard_map/while/body/eval_jaxpr/gqs,sd->qgd/dot_general | solution.py:67
  119.2 1.8 fusion.115
  121.0 1.9 copy-done.1
  123.0 1.1 fusion.116
  124.1 5.0 %fusion.117 = bf16[4,128,4,128]{1,3,2,0:T(8,128)(2,1)S(1)} fusion(bf16[4,128,4,128]{1,3,2,0:T(8,128)(2,1)S(1)} %get-tuple-element.178, s32[]{:T(128)} %get-tuple-element.177, f32[4,128]{1,0:T(4,128)S(1)} %fusion.116, bf16[2048,4,128]{0,2,1:T(8,128)(2,1)} %get-tuple-element.190, s32[]{:T(128)S(6)} %select_n.109, f32[2048,128,4]{1,0,2:T(8,128)} %copy-done.1), kind=kOutput, calls=%fused_computation.14.clone.1 | convolution fusion | flops 273746432 | bytes 9046532 | tf_op jit(solution)/shard_map/while/body/eval_jaxpr/gqs,sd->qgd/dot_general | solution.py:67
  129.1 4.8 %multiply_reduce_fusion.2 = (f32[128]{0:T(128)S(1)}, f32[128,2048]{1,0:T(8,128)S(1)}) fusion(bf16[128,2048]{0,1:T(8,128)(2,1)S(1)} %bitcast.181, bf16[2048,2048]{1,0:T(8,128)(2,1)} %param.23), kind=kOutput, calls=%fused_computation.65 | convolution fusion | flops 1074790272 | bytes 9961984 | tf_op jit(solution)/shard_map/dot_general | solution.py:128
  134.6 3.3 %gather_fusion = bf16[512,2048]{1,0:T(8,128)(2,1)} fusion(bf16[129,2048]{1,0:T(8,128)(2,1)S(1)} %concatenate.35, s32[1024]{0:T(1024)S(1)} %pad_clamp_fusion.1), kind=kCustom, calls=%fused_computation | custom fusion | bytes 4196352 | tf_op jit(solution)/shard_map/gather | solution.py:148
  137.9 4.1 %reshape.477 = bf16[128,1,4,2048]{3,2,0,1:T(4,128)(2,1)} reshape(bf16[512,2048]{1,0:T(8,128)(2,1)} %gather_fusion) | data formatting | bytes 4194304 | tf_op jit(solution)/shard_map/reshape | solution.py:149
  142.0 38.3 %all_to_all.10 = bf16[128,1,4,2048]{3,2,1,0:T(4,128)(2,1)S(1)} all-to-all(bf16[128,1,4,2048]{3,2,1,0:T(4,128)(2,1)} %bitcast.177), channel_id=1, replica_groups=mesh['sp'=16,'dp'=8] {'sp','dp'}, dimensions={0} | all-to-all | bytes 4194304 | tf_op jit(solution)/shard_map/all_to_all | solution.py:151
  180.3 1.3 copy-done.4
  181.6 3.4 %fusion.41 = f32[128,1,4,512]{3,0,2,1:T(8,128)} fusion(bf16[1,2048,512]{2,1,0:T(8,128)(2,1)S(1)} %copy-done.14, bf16[128,1,4,2048]{3,2,1,0:T(4,128)(2,1)S(1)} %all_to_all.10), kind=kOutput, calls=%fused_computation.52 | convolution fusion | flops 1073741824 | bytes 5242880 | tf_op jit(solution)/shard_map/nesd,edf->nesf/dot_general | solution.py:86
  185.0 7.5 %fusion.30 = bf16[128,1,4,2048]{3,0,2,1:T(8,128)(2,1)} fusion(bf16[1,512,2048]{2,1,0:T(8,128)(2,1)S(1)} %copy-done, bf16[1,2048,512]{2,1,0:T(8,128)(2,1)} %param.30, bf16[128,1,4,2048]{3,2,1,0:T(4,128)(2,1)} %copy-done.4, f32[128,1,4,512]{3,0,2,1:T(8,128)} %fusion.41), kind=kOutput, calls=%fused_computation.34 | convolution fusion | flops 2150105088 | bytes 9437184 | tf_op jit(solution)/shard_map/nesf,efd->nesd/dot_general | solution.py:89
  192.6 4.5 %copy.49 = bf16[128,1,4,2048]{3,2,1,0:T(4,128)(2,1)} copy(bf16[128,1,4,2048]{3,0,2,1:T(8,128)(2,1)} %fusion.30) | data formatting | bytes 4194304 | tf_op jit(solution)/shard_map/convert_element_type | solution.py:91
  197.1 6.0 %all-to-all-start.1 = ((bf16[128,1,4,2048]{3,2,1,0:T(4,128)(2,1)}), bf16[128,1,4,2048]{3,2,1,0:T(4,128)(2,1)}, u32[]{:S(2)}, u32[]{:S(2)}) async-start(bf16[128,1,4,2048]{3,2,1,0:T(4,128)(2,1)} %copy.49), calls=%async_computation.1 | async-start | bytes 4194304 | tf_op jit(solution)/shard_map/all_to_all | solution.py:156
  203.3 29.5 %all-to-all-done.1 = bf16[128,1,4,2048]{3,2,1,0:T(4,128)(2,1)} async-done(((bf16[128,1,4,2048]{3,2,1,0:T(4,128)(2,1)}), bf16[128,1,4,2048]{3,2,1,0:T(4,128)(2,1)}, u32[]{:S(2)}, u32[]{:S(2)}) %all-to-all-start.1) | async-done | bytes 2097184 | tf_op jit(solution)/shard_map/all_to_all | solution.py:156
  232.8 4.0 %reshape.483 = bf16[512,2048]{1,0:T(8,128)(2,1)} reshape(bf16[128,1,4,2048]{3,2,1,0:T(4,128)(2,1)} %all-to-all-done.1) | data formatting | bytes 4194304 | tf_op jit(solution)/shard_map/reshape | solution.py:158
  236.7 5.2 %gather_fusion.1 = bf16[256,2048]{1,0:T(8,128)(2,1)} fusion(bf16[512,2048]{1,0:T(8,128)(2,1)} %reshape.483, s32[1024]{0:T(1024)S(1)} %pad_clamp_fusion), kind=kCustom, calls=%fused_computation.1 | custom fusion | bytes 2098176 | tf_op jit(solution)/shard_map/gather | solution.py:158
  241.9 3.4 %reshape.490 = f32[128,2,2048]{2,1,0:T(2,128)} reshape(bf16[256,2048]{1,0:T(8,128)(2,1)} %gather_fusion.1) | data formatting | bytes 3145728 | tf_op jit(solution)/shard_map/convert_element_type | solution.py:159
  245.3 4.8 %multiply_reduce_fusion.1 = f32[128,2048]{1,0:T(8,128)S(1)} fusion(f32[128,2,2048]{2,1,0:T(2,128)} %reshape.490, f32[128,2]{1,0:T(8,128)S(1)} %copy.41), kind=kLoop, calls=%fused_computation.46 | loop fusion | flops 786432 | bytes 3146752 | tf_op jit(solution)/shard_map/reduce_sum | solution.py:164
  250.2 0.9 fusion.77
  (81 shorter events, 8.2 us)
Async XLA Ops:
  6.5 178.5 %copy-start = (bf16[1,512,2048]{2,1,0:T(8,128)(2,1)S(1)}, bf16[1,512,2048]{2,1,0:T(8,128)(2,1)}, u32[]{:S(2)}) copy-start(bf16[1,512,2048]{2,1,0:T(8,128)(2,1)} %param.31) | copy-start | bytes 6291460
  6.5 9.1 %copy-start.9 = (s32[1,128,2]{1,2,0:T(2,128)S(1)}, s32[1,128,2]{1,2,0:T(2,128)}, u32[]{:S(2)}) copy-start(s32[1,128,2]{1,2,0:T(2,128)} %param.26) | copy-start | bytes 3076
  6.5 62.6 %all-gather.2.cloned.1.call-start = ((), (), s32[]{:S(2)}) async-start(), calls=%async_computation.2 | async-start | bytes 4456448 | tf_op jit(solution)/shard_map/all_gather | solution.py:21
  21.7 4.9 %copy-start.10 = (f32[128]{0:T(128)S(1)}, f32[128]{0:T(128)}, u32[]{:S(2)}) copy-start(f32[128]{0:T(128)} %param.21) | copy-start | bytes 1540
  75.2 1.2 copy-start.2
  75.2 1.5 copy-start.3
  75.2 1.5 copy-start.11
  76.7 2.8 %copy-start.5 = (bf16[4,128,4,128]{1,3,2,0:T(8,128)(2,1)S(1)}, bf16[4,128,4,128]{1,3,2,0:T(8,128)(2,1)}, u32[]{:S(2)}) copy-start(bf16[4,128,4,128]{1,3,2,0:T(8,128)(2,1)} %custom-call.4) | copy-start | bytes 1572868
  83.9 1.9 copy-start.1
  96.3 1.9 copy-start.1
  108.6 1.9 copy-start.1
  121.0 1.9 copy-start.1
  129.1 4.8 %copy-start.6 = (bf16[1,128,2048]{2,1,0:T(8,128)(2,1)S(1)}, bf16[1,128,2048]{2,1,0:T(8,128)(2,1)}, u32[]{:S(2)}) copy-start(bf16[1,128,2048]{2,1,0:T(8,128)(2,1)} %param.17) | copy-start | bytes 1572868
  129.1 4.8 %copy-start.7 = (f32[2048]{0:T(1024)S(1)}, f32[2048]{0:T(1024)}, u32[]{:S(2)}) copy-start(f32[2048]{0:T(1024)} %param.24) | copy-start | bytes 24580
  129.1 5.2 %copy-start.8 = (f32[2048]{0:T(1024)S(1)}, f32[2048]{0:T(1024)}, u32[]{:S(2)}) copy-start(f32[2048]{0:T(1024)} %param.25) | copy-start | bytes 24580
  142.0 39.6 %copy-start.14 = (bf16[1,2048,512]{2,1,0:T(8,128)(2,1)S(1)}, bf16[1,2048,512]{2,1,0:T(8,128)(2,1)}, u32[]{:S(2)}) copy-start(bf16[1,2048,512]{2,1,0:T(8,128)(2,1)} %param.29) | copy-start | bytes 6291460
  180.3 1.3 copy-start.4
  192.5 10.6 %copy-start.12 = (f32[1,128]{1,0:T(1,128)S(1)}, f32[1,128]{1,0:T(1,128)}, u32[]{:S(2)}) copy-start(f32[1,128]{1,0:T(1,128)} %param.28) | copy-start | bytes 1540
  192.6 10.6 %copy-start.13 = (f32[1,128]{1,0:T(1,128)S(1)}, f32[1,128]{1,0:T(1,128)}, u32[]{:S(2)}) copy-start(f32[1,128]{1,0:T(1,128)} %param.27) | copy-start | bytes 1540
  197.1 35.7 %all-to-all-start.1 = ((bf16[128,1,4,2048]{3,2,1,0:T(4,128)(2,1)}), bf16[128,1,4,2048]{3,2,1,0:T(4,128)(2,1)}, u32[]{:S(2)}, u32[]{:S(2)}) async-start(bf16[128,1,4,2048]{3,2,1,0:T(4,128)(2,1)} %copy.49), calls=%async_computation.1 | async-start | bytes 4194304 | tf_op jit(solution)/shard_map/all_to_all | solution.py:156
Sparse Core Ops, SparseCore 0:
  9.6 59.4 all-gather.1
where the time goes:
time: 259 us; the launch traced here: 258 us
  waiting for transfers between devices  70.9 us (27%)
  local copies, waits for them, and re-layouts  46.1 us (18%)
  matrix products  42.7 us (16%)
  blocking collectives  38.3 us (15%)
  other arithmetic  32.2 us (12%)
  between operations  13.8 us (5%)
  loops' own time  7.97 us (3%)
  starting transfers between devices  6.04 us (2%)
    all_gather x1, waiting for transfers between devices, side_by_side(): lax.all_gather(both, axis, axis=dim, tiled=True)  41.4 us
    all_to_all x1, blocking collectives, local(): lax.all_to_all(shaped, ('sp', 'dp'), split_axis=0, concat_axis=0, tiled=T...  38.3 us
    all_to_all x1, waiting for transfers between devices, local(): lax.all_to_all(answered, ('sp', 'dp'), split_axis=0, concat_axis=0, tiled...  29.5 us
    dot_general x4, matrix products, one_item(): jnp.einsum('gqs,sd->qgd', weights, value_block, preferred_element_type=jn...  19.8 us
    another operation x1, loops' own time, attend_blocks(): results = lax.map(one_item, jnp.arange(blocks * kv_count, dtype=jnp.int32))  7.97 us
    while x8, local copies, waits for them, and re-layouts  7.68 us
    unnamed x33, local copies, waits for them, and re-layouts  7.64 us
    dot_general x1, matrix products, expert_ffn(): jnp.einsum('nesf,efd->nesd', hidden, down_weight, preferred_element_type=...  7.52 us
  transfers between devices with their start and end apart: 2, of which 2 were waited for; matrix products, arithmetic and copies ran while one was open for 7% of the time, Pallas kernels for 0%

commit v1 on v0

v1 whole, which is shorter than its diff:
```python
import functools

import jax
import jax.numpy as jnp
import numpy as np
from jax import lax
from jax.experimental import pallas as pl
from jax.experimental.pallas import tpu as pltpu
from jax.sharding import Mesh
from jax.sharding import PartitionSpec as P

HEADS = 16
KV_HEADS = 4
HEAD_DIM = 128
GRID_W = 64
CAP = 4
EPSILON = 1e-06
F32 = jnp.float32
BF16 = jnp.bfloat16


def dot(a, b, dims=((1,), (0,))):
    return lax.dot_general(a, b, (dims, ((), ())), preferred_element_type=F32)


def pack_kernel(place_ref, q_ref, k_ref, v_ref, qg_ref, kg_ref, inv_ref, out_ref, cos_ref, sin_ref):
    tokens = k_ref.shape[0]
    shape = (tokens, HEAD_DIM)
    lane = lax.broadcasted_iota(jnp.int32, shape, 1)
    first = lax.bitwise_and(lane, 32) == 0

    @pl.when(pl.program_id(0) == 0)
    def _():
        position = place_ref[0] * tokens + lax.broadcasted_iota(jnp.int32, shape, 0)
        grid_row = lax.shift_right_logical(position, 6)
        grid_col = lax.bitwise_and(position, GRID_W - 1)
        angles = jnp.where(lane < HEAD_DIM // 2, grid_row, grid_col).astype(F32) * inv_ref[...]
        sin = jnp.sin(angles)
        cos_ref[...] = jnp.cos(angles)
        sin_ref[...] = jnp.where(first, -sin, sin)

    cos = cos_ref[...]
    sin = sin_ref[...]

    def turned(raw, gain):
        floats = raw.astype(F32)
        mean = jnp.mean(floats * floats, axis=-1, keepdims=True)
        normed = floats * lax.rsqrt(mean + EPSILON) * gain
        other = jnp.where(first, pltpu.roll(normed, 96, 1), pltpu.roll(normed, 32, 1))
        return (normed * cos + other * sin).astype(BF16)

    key = turned(k_ref[...], kg_ref[...])
    value = v_ref[...]
    for h in range(out_ref.shape[0]):
        query = turned(q_ref[:, h * HEAD_DIM : (h + 1) * HEAD_DIM], qg_ref[...])
        out_ref[h, :, 0:HEAD_DIM] = query
        out_ref[h, :, HEAD_DIM : 2 * HEAD_DIM] = key
        out_ref[h, :, 2 * HEAD_DIM : 3 * HEAD_DIM] = value


def attend_kernel(x_ref, out_ref, value_ref, even_ref, odd_ref):
    length = x_ref.shape[0]
    block = even_ref.shape[0]
    blocks = length // block
    value_ref[:, 0:HEAD_DIM] = x_ref[:, 2 * HEAD_DIM : 3 * HEAD_DIM]
    value_ref[:, HEAD_DIM:] = jnp.ones((length, HEAD_DIM), BF16)
    scale = float(HEAD_DIM ** (-0.5) * np.log2(np.e))

    def score(i, score_ref):
        rows = pl.ds(pl.multiple_of(i * block, block), block)
        score_ref[...] = dot(x_ref[rows, 0:HEAD_DIM], x_ref[:, HEAD_DIM : 2 * HEAD_DIM], ((1,), (1,)))

    def mix(i, score_ref):
        rows = pl.ds(pl.multiple_of(i * block, block), block)
        top = jnp.max(score_ref[...], axis=-1, keepdims=True)
        weights = jnp.exp2((score_ref[...] - top) * scale).astype(BF16)
        both = dot(weights, value_ref[...])
        out_ref[rows, :] = (both[:, 0:HEAD_DIM] / both[:, HEAD_DIM:]).astype(BF16)

    score(0, even_ref)

    def two(j, carry):
        i = 2 * j
        score(i + 1, odd_ref)
        mix(i, even_ref)
        score(jnp.minimum(i + 2, blocks - 1), even_ref)
        mix(i + 1, odd_ref)
        return carry

    lax.fori_loop(0, blocks // 2, two, 0)


def rms(floats, gain):
    return floats * lax.rsqrt(jnp.mean(floats * floats, axis=-1, keepdims=True) + EPSILON) * gain


def proj_kernel(place_ref, att_ref, w_ref, res_ref, post_ref, pre_ref, ids_ref, *rest):
    *_, out_ref, stream_ref, slot_ref, x_ref = rest
    tokens, width = x_ref.shape
    for h in range(HEADS):
        x_ref[:, h * HEAD_DIM : (h + 1) * HEAD_DIM] = att_ref[h]
    experts = 2 * out_ref.shape[0]
    which = lax.broadcasted_iota(jnp.int32, (experts, tokens), 0)
    first = ids_ref[0:1, :]
    second = ids_ref[1:2, :]
    hit_first = jnp.where(which == first, 1.0, 0.0)
    hit_second = jnp.where(which == second, 1.0, 0.0)
    row = lax.broadcasted_iota(jnp.int32, (tokens, tokens), 0)
    col = lax.broadcasted_iota(jnp.int32, (tokens, tokens), 1)
    before = jnp.where(row < col, 1.0, 0.0).astype(BF16)
    rank = dot((hit_first + hit_second).astype(BF16), before)
    rank_first = jnp.sum(rank * hit_first, axis=0, keepdims=True).astype(jnp.int32)
    rank_second = jnp.sum(rank * hit_second, axis=0, keepdims=True).astype(jnp.int32)
    core = place_ref[1]

    def slot_of(expert, rank):
        side = lax.bitwise_xor(lax.bitwise_and(expert, 1), core)
        return lax.shift_right_logical(expert, 1) * (2 * CAP) + rank * 2 + side

    slot_first = slot_of(first, rank_first)
    slot_second = slot_of(second, rank_second)
    slot_ref[0:1, :] = slot_first
    slot_ref[1:2, :] = slot_second
    slot = lax.broadcasted_iota(jnp.int32, (experts * CAP, tokens), 0)
    here = (slot == slot_first) | (slot == slot_second)
    picks = jnp.where(here, 1.0, 0.0).astype(BF16)
    mixed = dot(x_ref[...], w_ref[...]).astype(BF16).astype(F32)
    stream = (res_ref[...].astype(F32) + rms(mixed, post_ref[...])).astype(BF16)
    stream_ref[...] = stream
    normed = rms(stream.astype(F32), pre_ref[...]).astype(BF16)
    out_ref[...] = dot(picks, normed).astype(BF16).reshape(out_ref.shape)


def expert_kernel(y_ref, *rest):
    *weights, out_ref, wide_ref, x_ref = rest
    slots, width = y_ref.shape
    sides = [pl.ds(side, slots // 2, stride=2) for side in range(2)]
    blocks = [slice(c * 128, (c + 1) * 128) for c in range(width // 128)]
    for c, cols in enumerate(blocks):
        wide_ref[c] = y_ref[:, cols].astype(F32)
        for side in range(2):
            x_ref[side, :, cols] = wide_ref[c, sides[side], :].astype(BF16)
    for side in range(2):
        gate_ref, up_ref, down_ref = weights[3 * side : 3 * side + 3]
        gated = dot(x_ref[side], gate_ref[...])
        lifted = dot(x_ref[side], up_ref[...])
        hidden = (gated / (1.0 + jnp.exp(-gated)) * lifted).astype(BF16)
        made = dot(hidden, down_ref[...])
        for c, cols in enumerate(blocks):
            wide_ref[c, sides[side], :] = made[:, cols]
    for c, cols in enumerate(blocks):
        out_ref[:, cols] = wide_ref[c].astype(BF16)


def combine_kernel(z_ref, stream_ref, slot_ref, weight_ref, share_ref, out_ref):
    slots = z_ref.shape[0]
    tokens, width = stream_ref.shape
    slot = lax.broadcasted_iota(jnp.int32, (slots, tokens), 0)
    picks = [jnp.where(slot == slot_ref[i : i + 1, :], 1.0, 0.0).astype(BF16) for i in range(2)]
    picked = dot(jnp.concatenate(picks, axis=1), z_ref[...], ((0,), (0,)))
    column = lambda row: jnp.broadcast_to(row, (tokens, tokens)).T[:, 0:1]
    weight = weight_ref[...]
    share = share_ref[...]
    weight_first = column(weight * share)
    weight_second = column(weight * (1.0 - share))
    ffn = weight_first * picked[0:tokens] + weight_second * picked[tokens:]
    out_ref[...] = (stream_ref[...].astype(F32) + ffn).astype(BF16)


def local(
    residual_in,
    query_proj,
    key_proj,
    value_proj,
    query_gain,
    key_gain,
    out_weight,
    post_gain,
    pre_gain,
    route_ids,
    group_weight,
    first_share,
    gate_weight,
    up_weight,
    down_weight,
):
    sp_count = lax.axis_size("sp")
    tokens, width = query_proj.shape[1:]
    length = tokens * sp_count
    chips = sp_count * lax.axis_size("y")
    experts = 2 * chips
    assert sp_count == HEADS and gate_weight.shape[0] == 1 and lax.axis_size("core") == 2
    quarter = HEAD_DIM // 4
    inverse = np.float32(10000.0) ** (-np.arange(quarter, dtype=np.float32) / np.float32(quarter))
    inverse = jnp.asarray(np.tile(inverse.astype(np.float32), 4)[None])
    place = jnp.stack([lax.axis_index("sp"), lax.axis_index("core")]).astype(jnp.int32)
    swap = [(0, 1), (1, 0)]
    own = (gate_weight[0], up_weight[0], down_weight[0])
    partner = tuple(lax.ppermute(one, "core", swap) for one in own)

    vmem = pl.BlockSpec(memory_space=pltpu.VMEM)
    smem = pl.BlockSpec(memory_space=pltpu.SMEM)
    limit = lambda mib: pltpu.CompilerParams(vmem_limit_bytes=mib * 2**20)
    group = HEADS // KV_HEADS
    fixed = lambda *shape: pl.BlockSpec(shape, lambda n: (0,) * len(shape))
    packed = pl.pallas_call(
        pack_kernel,
        grid=(KV_HEADS,),
        out_shape=jax.ShapeDtypeStruct((HEADS, tokens, 3 * HEAD_DIM), BF16),
        in_specs=[
            smem,
            pl.BlockSpec((tokens, group * HEAD_DIM), lambda n: (0, n)),
            pl.BlockSpec((tokens, HEAD_DIM), lambda n: (0, n)),
            pl.BlockSpec((tokens, HEAD_DIM), lambda n: (0, n)),
            fixed(1, HEAD_DIM),
            fixed(1, HEAD_DIM),
            fixed(1, HEAD_DIM),
        ],
        out_specs=pl.BlockSpec((group, tokens, 3 * HEAD_DIM), lambda n: (n, 0, 0)),
        scratch_shapes=[pltpu.VMEM((tokens, HEAD_DIM), F32)] * 2,
        compiler_params=limit(63),
        name="pack",
    )(place, query_proj[0], key_proj[0], value_proj[0], query_gain[None], key_gain[None], inverse)
    gathered = lax.all_to_all(packed, "sp", 0, 0, tiled=True)
    block = 512
    attended = pl.pallas_call(
        attend_kernel,
        out_shape=jax.ShapeDtypeStruct((length, HEAD_DIM), BF16),
        in_specs=[vmem],
        out_specs=vmem,
        scratch_shapes=[
            pltpu.VMEM((length, 2 * HEAD_DIM), BF16),
            pltpu.VMEM((block, length), F32),
            pltpu.VMEM((block, length), F32),
        ],
        compiler_params=limit(24),
        cost_estimate=pl.CostEstimate(
            flops=4 * length * length * HEAD_DIM * 4,
            bytes_accessed=length * HEAD_DIM * 8,
            transcendentals=length * length,
        ),
        name="attend",
    )(gathered.reshape(length, 3 * HEAD_DIM))
    attended = lax.all_to_all(attended.reshape(sp_count, tokens, HEAD_DIM), "sp", 0, 0, tiled=True)
    hbm = pl.BlockSpec(memory_space=pltpu.HBM)
    sent, stream, slots = pl.pallas_call(
        proj_kernel,
        out_shape=(
            jax.ShapeDtypeStruct((chips, 2 * CAP, width), BF16),
            jax.ShapeDtypeStruct((tokens, width), BF16),
            jax.ShapeDtypeStruct((8, tokens), jnp.int32),
        ),
        in_specs=[smem] + [vmem] * 6 + [hbm] * 3,
        out_specs=(vmem,) * 3,
        scratch_shapes=[
            pltpu.VMEM((tokens, width), BF16),
        ],
        compiler_params=limit(24),
        name="project",
    )(
        place,
        attended,
        out_weight,
        residual_in[0],
        post_gain[None],
        pre_gain[None],
        route_ids[0].T,
        *partner,
    )
    peers = ("sp", "y")
    arrived = lax.all_to_all(sent, peers, 0, 0, tiled=True)
    rows = experts * CAP
    answered = pl.pallas_call(
        expert_kernel,
        out_shape=jax.ShapeDtypeStruct((rows, width), BF16),
        in_specs=[vmem] * 7,
        out_specs=vmem,
        scratch_shapes=[
            pltpu.VMEM((width // 128, rows, 128), F32),
            pltpu.VMEM((2, rows // 2, width), BF16),
        ],
        compiler_params=limit(24),
        name="expert",
    )(arrived.reshape(rows, width), *own, *partner)
    returned = lax.all_to_all(answered.reshape(chips, 2 * CAP, width), peers, 0, 0, tiled=True)
    combined = pl.pallas_call(
        combine_kernel,
        out_shape=jax.ShapeDtypeStruct((tokens, width), BF16),
        in_specs=[vmem] * 5,
        out_specs=vmem,
        compiler_params=limit(16),
        name="combine",
    )(returned.reshape(rows, width), stream, slots, group_weight, first_share)
    return combined[None]


def solution(mesh):
    assert mesh.axis_names[0] == "sp"
    grid = mesh.devices.reshape(mesh.devices.shape[0], -1, 2)
    mesh = Mesh(grid, ("sp", "y", "core"))
    placed = (
        P(("y", "core"), "sp", None),
        P(("y", "core"), "sp", None),
        P(("y", "core"), "sp", None),
        P(("y", "core"), "sp", None),
        P(),
        P(),
        P(),
        P(),
        P(),
        P(("y", "core"), "sp", None),
        P(("y", "core"), "sp"),
        P(("y", "core"), "sp"),
        P(("sp", "y", "core"), None, None),
        P(("sp", "y", "core"), None, None),
        P(("sp", "y", "core"), None, None),
    )
    return jax.shard_map(
        local, mesh=mesh, in_specs=placed, out_specs=P(("y", "core"), "sp", None), check_vma=False
    )
```

time: 259 us -> 141 us (0.54)
  waiting for transfers between devices: 70.9 us -> 23.9 us
  local copies, waits for them, and re-layouts: 46.1 us -> 0.06 us
  blocking collectives: 38.3 us -> 83.2 us
  matrix products: 42.7 us -> 0 us
  other arithmetic: 32.2 us -> 0.64 us
  Pallas kernels: 0 us -> 23.5 us
  between operations: 13.8 us -> 0.18 us
  loops' own time: 7.97 us -> 0 us
  starting transfers between devices: 6.04 us -> 8.71 us
    all_to_all x1 -> x3, blocking collectives: 38.3 us -> 83.2 us  [the longest x1 35.8 us: local(): arrived = lax.all_to_all(sent, peers, 0, 0, tiled=True)]
    dot_general x11 -> x0, matrix products: 42.7 us -> none  [the longest x4 19.8 us: one_item(): jnp.einsum('gqs,sd->qgd', weights, value_block, preferred_element_type=jn...]
    all_gather x1 -> x0, waiting for transfers between devices: 41.4 us -> none  [side_by_side(): lax.all_gather(both, axis, axis=dim, tiled=True)]
    pallas_call x0 -> x5, Pallas kernels: none -> 23.5 us  [the longest x1 7.42 us: local(): pl.pallas_call(attend_kernel, out_shape=jax.ShapeDtypeStruct((length, HEA...]
    convert_element_type x7 -> x0, other arithmetic: 9.6 us -> none  [the longest x2 5.45 us: rotate_heads(): floats = raw_heads.astype(jnp.float32)]
    gather x2 -> x0, local copies, waits for them, and re-layouts: 8.54 us -> none  [the longest x1 5.2 us: local(): returned.reshape(expert_count * capacity, model_width)[slot_index]]
    reshape x2 -> x0, local copies, waits for them, and re-layouts: 8.08 us -> none  [the longest x1 4.12 us: local(): outgoing.reshape(sp_count * dp_count, local_experts, capacity, model_width)]
    another operation x1 -> x0, loops' own time: 7.97 us -> none  [attend_blocks(): results = lax.map(one_item, jnp.arange(blocks * kv_count, dtype=jnp.int32))]
  transfers between devices with their start and end apart: 2 -> 4, of which waited for: 2 -> 1; matrix products, arithmetic and copies ran while one was open for 7% -> 0% of each run, Pallas kernels for 0% -> 5%
where the time goes in v1:
time: 141 us; the launch traced here: 140 us
  blocking collectives  83.2 us (59%)
  waiting for transfers between devices  23.9 us (17%)
  Pallas kernels  23.5 us (17%)
  starting transfers between devices  8.71 us (6%)
    all_to_all x1, blocking collectives, local(): arrived = lax.all_to_all(sent, peers, 0, 0, tiled=True)  35.8 us
    all_to_all x1, blocking collectives, local(): lax.all_to_all(answered.reshape(chips, 2 * CAP, width), peers, 0, 0, tile...  33 us
    all_to_all x1, waiting for transfers between devices, local(): gathered = lax.all_to_all(packed, 'sp', 0, 0, tiled=True)  23.9 us
    all_to_all x1, blocking collectives, local(): lax.all_to_all(attended.reshape(sp_count, tokens, HEAD_DIM), 'sp', 0, 0,...  14.3 us
    all_to_all x1, starting transfers between devices, local(): gathered = lax.all_to_all(packed, 'sp', 0, 0, tiled=True)  8.03 us
    pallas_call x1, Pallas kernels, local(): pl.pallas_call(attend_kernel, out_shape=jax.ShapeDtypeStruct((length, HEA...  7.42 us
    pallas_call x1, Pallas kernels, local(): pl.pallas_call(expert_kernel, out_shape=jax.ShapeDtypeStruct((rows, width...  6.29 us
    pallas_call x1, Pallas kernels, local(): pl.pallas_call(pack_kernel, grid=(KV_HEADS,), out_shape=jax.ShapeDtypeStr...  5.23 us
  transfers between devices with their start and end apart: 4, of which 1 were waited for; matrix products, arithmetic and copies ran while one was open for 0% of the time, Pallas kernels for 5%

profile of v1, /device:TPU:0, one launch (start us, length us, event | category | flops | bytes accessed | tf_op | source)
XLA Modules:
  0.0 140.2 jit_solution(10864997376090157646)
XLA Ops:
  0.0 0.6 pad_add_fusion.place_ref
  0.6 5.2 %pack.1 = bf16[16,128,384]{2,1,0:T(8,128)(2,1)} custom-call(s32[2]{0:T(128)} %pad_add_fusion.place_ref, bf16[128,2048]{1,0:T(8,128)(2,1)} %bitcast.38, bf16[128,512]{1,0:T(8,128)(2,1)} %bitcast.39, bf16[128,512]{1,0:T(8,128)(2,1)} %bitcast.40, f32[1,128]{1,0:T(1,128)} %bitcast.41, f32[1,128]{1,0:T(1,128)} %bitcast.42, f32[1,128]{1,0:T(1,128)} %constant.12.clone.inv_ref), custom_call_target="tpu_custom_call" | custom-call | tf_op jit(solution)/shard_map/pack/pallas_call | solution.py:206
  5.9 8.0 %all-to-all-start = ((bf16[16,128,384]{2,1,0:T(8,128)(2,1)}), bf16[16,128,384]{2,1,0:T(8,128)(2,1)}, u32[]{:S(2)}, u32[]{:S(2)}) async-start(bf16[16,128,384]{2,1,0:T(8,128)(2,1)} %pack.1), calls=%async_computation | async-start | bytes 3145728 | tf_op jit(solution)/shard_map/all_to_all | solution.py:224
  13.9 0.1 collective-permute-start
  14.0 0.5 collective-permute-start.1
  14.5 0.1 collective-permute-start.2
  14.6 23.9 %all-to-all-done = bf16[16,128,384]{2,1,0:T(8,128)(2,1)} async-done(((bf16[16,128,384]{2,1,0:T(8,128)(2,1)}), bf16[16,128,384]{2,1,0:T(8,128)(2,1)}, u32[]{:S(2)}, u32[]{:S(2)}) %all-to-all-start) | async-done | bytes 1572896 | tf_op jit(solution)/shard_map/all_to_all | solution.py:224
  38.5 0.0 slice-start
  38.5 0.0 slice-start.1
  38.5 0.0 copy-start.3
  38.5 0.0 copy-start.4
  38.5 0.0 copy-start.5
  38.5 0.0 copy-start.6
  38.5 0.0 copy-start.7
  38.5 7.4 %attend.1 = bf16[2048,128]{1,0:T(8,128)(2,1)S(1)} custom-call(bf16[2048,384]{1,0:T(8,128)(2,1)} %bitcast.7.x_ref), custom_call_target="tpu_custom_call" | custom-call | flops 8589934592 | bytes 2097152 | tf_op jit(solution)/shard_map/attend/pallas_call | solution.py:226
  46.0 14.3 %all_to_all.20.att_ref = bf16[16,128,128]{2,1,0:T(8,128)(2,1)S(1)} all-to-all(bf16[16,128,128]{2,1,0:T(8,128)(2,1)S(1)} %bitcast.34), channel_id=1, replica_groups=mesh['sp'=16,'y'=4,'core'=2] {'sp'}, dimensions={0} | all-to-all | bytes 1048576 | tf_op jit(solution)/shard_map/all_to_all | solution.py:244
  60.3 0.0 collective-permute-done.rest_0_.rest_3_
  60.3 0.0 collective-permute-done.1.rest_1_.rest_4_
  60.3 0.0 collective-permute-done.2.rest_2_.rest_5_
  60.3 0.0 slice-done
  60.3 0.0 slice-done.1
  60.3 0.0 copy-done.3
  60.4 0.0 copy-done.4
  60.4 0.0 copy-done.5
  60.4 0.0 copy-done.6
  60.4 0.0 copy-done.7
  60.4 0.0 copy-start.2
  60.4 3.0 %project.1 = (bf16[64,8,2048]{2,1,0:T(8,128)(2,1)S(1)}, bf16[128,2048]{1,0:T(8,128)(2,1)S(1)}, s32[8,128]{1,0:T(8,128)S(1)}) custom-call(s32[2]{0:T(128)S(1)} %copy-done.6, bf16[16,128,128]{2,1,0:T(8,128)(2,1)S(1)} %all_to_all.20.att_ref, bf16[2048,2048]{1,0:T(8,128)(2,1)S(1)} %bitcast.23, bf16[128,2048]{1,0:T(8,128)(2,1)S(1)} %bitcast.33, ...), custom_call_target="tpu_custom_call" | custom-call | tf_op jit(solution)/shard_map/project/pallas_call | solution.py:246
  63.4 0.0 copy-start
  63.4 0.0 copy-start.1
  63.4 35.8 %all_to_all.21 = bf16[64,8,2048]{2,1,0:T(8,128)(2,1)S(1)} all-to-all(bf16[64,8,2048]{2,1,0:T(8,128)(2,1)S(1)} %get-tuple-element.8), channel_id=1, replica_groups=mesh['sp'=16,'y'=4,'core'=2] {'sp','y'}, dimensions={0} | all-to-all | bytes 4194304 | tf_op jit(solution)/shard_map/all_to_all | solution.py:271
  99.2 0.0 copy-done.2
  99.2 0.0 copy-done
  99.2 0.0 copy-done.1
  99.2 6.3 %expert.1 = bf16[512,2048]{1,0:T(8,128)(2,1)S(1)} custom-call(bf16[512,2048]{1,0:T(8,128)(2,1)S(1)} %bitcast.25, bf16[2048,512]{1,0:T(8,128)(2,1)S(1)} %bitcast.28, bf16[2048,512]{1,0:T(8,128)(2,1)S(1)} %bitcast.30, bf16[512,2048]{1,0:T(8,128)(2,1)S(1)} %bitcast.32, bf16[2048,512]{1,0:T(8,128)(2,1)S(1)} %collective-permute-done.rest_0_.rest_3_, ...), custom_call_target="tpu_custom_call" | custom-call | tf_op jit(solution)/shard_map/expert/pallas_call | solution.py:273
  105.5 0.0 copy-start.8
  105.5 0.0 copy-start.9
  105.5 33.0 %all_to_all.22 = bf16[64,8,2048]{2,1,0:T(8,128)(2,1)S(1)} all-to-all(bf16[64,8,2048]{2,1,0:T(8,128)(2,1)S(1)} %bitcast.26), channel_id=1, replica_groups=mesh['sp'=16,'y'=4,'core'=2] {'sp','y'}, dimensions={0} | all-to-all | bytes 4194304 | tf_op jit(solution)/shard_map/all_to_all | solution.py:285
  138.6 0.0 copy-done.8
  138.6 0.0 copy-done.9
  138.6 1.6 %combine.1 = bf16[128,2048]{1,0:T(8,128)(2,1)} custom-call(bf16[512,2048]{1,0:T(8,128)(2,1)S(1)} %bitcast.24, bf16[128,2048]{1,0:T(8,128)(2,1)S(1)} %get-tuple-element.9.stream_ref, s32[8,128]{1,0:T(8,128)S(1)} %get-tuple-element.10.slot_ref, f32[1,128]{1,0:T(1,128)S(1)} %copy-done.8, f32[1,128]{1,0:T(1,128)S(1)} %copy-done.9), custom_call_target="tpu_custom_call" | custom-call | tf_op jit(solution)/shard_map/combine/pallas_call | solution.py:286
  (1 shorter events, 0.0 us)
Async XLA Ops:
  5.9 32.6 %all-to-all-start = ((bf16[16,128,384]{2,1,0:T(8,128)(2,1)}), bf16[16,128,384]{2,1,0:T(8,128)(2,1)}, u32[]{:S(2)}, u32[]{:S(2)}) async-start(bf16[16,128,384]{2,1,0:T(8,128)(2,1)} %pack.1), calls=%async_computation | async-start | bytes 3145728 | tf_op jit(solution)/shard_map/all_to_all | solution.py:224
  13.9 46.4 %collective-permute-start = (bf16[2048,512]{1,0:T(8,128)(2,1)}, bf16[2048,512]{1,0:T(8,128)(2,1)S(1)}, u32[]{:S(2)}, u32[]{:S(2)}) collective-permute-start(bf16[2048,512]{1,0:T(8,128)(2,1)} %bitcast.27), channel_id=1, source_target_pairs={{0,1},{1,0},{2,3},{3,2},{4,5},{5,4},{6,7},{7,6},{8,9},{9,8},{10,11... | collective-permute-start | bytes 6291464 | tf_op jit(solution)/shard_map/ppermute | solution.py:199
  14.0 46.3 %collective-permute-start.1 = (bf16[2048,512]{1,0:T(8,128)(2,1)}, bf16[2048,512]{1,0:T(8,128)(2,1)}, u32[]{:S(2)}, u32[]{:S(2)}) collective-permute-start(bf16[2048,512]{1,0:T(8,128)(2,1)} %bitcast.29), channel_id=1, source_target_pairs={{0,1},{1,0},{2,3},{3,2},{4,5},{5,4},{6,7},{7,6},{8,9},{9,8},{10,11... | collective-permute-start | bytes 6291464 | tf_op jit(solution)/shard_map/ppermute | solution.py:199
  14.5 45.8 %collective-permute-start.2 = (bf16[512,2048]{1,0:T(8,128)(2,1)}, bf16[512,2048]{1,0:T(8,128)(2,1)}, u32[]{:S(2)}, u32[]{:S(2)}) collective-permute-start(bf16[512,2048]{1,0:T(8,128)(2,1)} %bitcast.31), channel_id=1, source_target_pairs={{0,1},{1,0},{2,3},{3,2},{4,5},{5,4},{6,7},{7,6},{8,9},{9,8},{10,11... | collective-permute-start | bytes 6291464 | tf_op jit(solution)/shard_map/ppermute | solution.py:199
  38.5 21.8 %slice-start = ((s8[8388608]{0:T(1024)(128)(4,1)}), s8[4194304]{0:T(1024)(128)(4,1)S(1)}, s32[]{:S(2)}) async-start(s8[8388608]{0:T(1024)(128)(4,1)} %bitcast.22), calls=%async_computation.4 | async-start | bytes 8388608
  38.5 21.8 %slice-start.1 = ((s8[8388608]{0:T(1024)(128)(4,1)}), s8[4194304]{0:T(1024)(128)(4,1)S(1)}, s32[]{:S(2)}) async-start(s8[8388608]{0:T(1024)(128)(4,1)} %bitcast.22), calls=%async_computation.5 | async-start | bytes 8388608
  38.5 21.9 %copy-start.3 = (bf16[1,128,2048]{2,1,0:T(8,128)(2,1)S(1)}, bf16[1,128,2048]{2,1,0:T(8,128)(2,1)}, u32[]{:S(2)}) copy-start(bf16[1,128,2048]{2,1,0:T(8,128)(2,1)} %param.16) | copy-start | bytes 1572868
  38.5 21.9 %copy-start.4 = (f32[2048]{0:T(1024)S(1)}, f32[2048]{0:T(1024)}, u32[]{:S(2)}) copy-start(f32[2048]{0:T(1024)} %param.23) | copy-start | bytes 24580
  38.5 21.9 %copy-start.5 = (f32[2048]{0:T(1024)S(1)}, f32[2048]{0:T(1024)}, u32[]{:S(2)}) copy-start(f32[2048]{0:T(1024)} %param.24) | copy-start | bytes 24580
  38.5 21.9 %copy-start.6 = (s32[2]{0:T(128)S(1)}, s32[2]{0:T(128)}, u32[]{:S(2)}) copy-start(s32[2]{0:T(128)} %pad_add_fusion.place_ref) | copy-start | bytes 28
  38.5 21.9 %copy-start.7 = (s32[1,128,2]{1,2,0:T(2,128)S(1)}, s32[1,128,2]{1,2,0:T(2,128)}, u32[]{:S(2)}) copy-start(s32[1,128,2]{1,2,0:T(2,128)} %param.25) | copy-start | bytes 3076
  60.4 38.8 %copy-start.2 = (bf16[1,512,2048]{2,1,0:T(8,128)(2,1)S(1)}, bf16[1,512,2048]{2,1,0:T(8,128)(2,1)}, u32[]{:S(2)}) copy-start(bf16[1,512,2048]{2,1,0:T(8,128)(2,1)} %param.30) | copy-start | bytes 6291460
  63.4 35.8 %copy-start = (bf16[1,2048,512]{2,1,0:T(8,128)(2,1)S(1)}, bf16[1,2048,512]{2,1,0:T(8,128)(2,1)}, u32[]{:S(2)}) copy-start(bf16[1,2048,512]{2,1,0:T(8,128)(2,1)} %param.28) | copy-start | bytes 6291460
  63.4 35.8 %copy-start.1 = (bf16[1,2048,512]{2,1,0:T(8,128)(2,1)S(1)}, bf16[1,2048,512]{2,1,0:T(8,128)(2,1)}, u32[]{:S(2)}) copy-start(bf16[1,2048,512]{2,1,0:T(8,128)(2,1)} %param.29) | copy-start | bytes 6291460
  105.5 33.1 %copy-start.8 = (f32[1,128]{1,0:T(1,128)S(1)}, f32[1,128]{1,0:T(1,128)}, u32[]{:S(2)}) copy-start(f32[1,128]{1,0:T(1,128)} %weight_ref.1) | copy-start | bytes 1540
  105.5 33.0 %copy-start.9 = (f32[1,128]{1,0:T(1,128)S(1)}, f32[1,128]{1,0:T(1,128)}, u32[]{:S(2)}) copy-start(f32[1,128]{1,0:T(1,128)} %share_ref.1) | copy-start | bytes 1540

commit v2 on v1

--- a/solution.py
+++ b/solution.py
@@ -23,39 +23,66 @@
     return lax.dot_general(a, b, (dims, ((), ())), preferred_element_type=F32)
 
 
-def pack_kernel(place_ref, q_ref, k_ref, v_ref, qg_ref, kg_ref, inv_ref, out_ref, cos_ref, sin_ref):
+def angle_tables(count):
+    quarter = HEAD_DIM // 4
+    inverse = np.float32(10000.0) ** (-np.arange(quarter, dtype=np.float32) / np.float32(quarter))
+    angles = np.arange(count, dtype=np.float32)[:, None] * inverse.astype(np.float32)
+    angles = np.tile(angles.astype(np.float64), (1, 4))
+    return np.stack([np.cos(angles), np.sin(angles)]).astype(np.float32)
+
+
+def partner_matrix():
+    lane = np.arange(HEAD_DIM)
+    low = (lane & 32) == 0
+    matrix = np.zeros((HEAD_DIM, HEAD_DIM), np.float32)
+    matrix[np.where(low, lane + 32, lane - 32), lane] = np.where(low, -1.0, 1.0)
+    return matrix
+
+
+def pack_kernel(
+    place_ref, q_ref, k_ref, v_ref, qg_ref, kg_ref, row_ref, col_ref, swap_ref, out_ref, table_ref
+):
     tokens = k_ref.shape[0]
-    shape = (tokens, HEAD_DIM)
-    lane = lax.broadcasted_iota(jnp.int32, shape, 1)
-    first = lax.bitwise_and(lane, 32) == 0
+    group = out_ref.shape[0]
 
     @pl.when(pl.program_id(0) == 0)
     def _():
-        position = place_ref[0] * tokens + lax.broadcasted_iota(jnp.int32, shape, 0)
-        grid_row = lax.shift_right_logical(position, 6)
-        grid_col = lax.bitwise_and(position, GRID_W - 1)
-        angles = jnp.where(lane < HEAD_DIM // 2, grid_row, grid_col).astype(F32) * inv_ref[...]
-        sin = jnp.sin(angles)
-        cos_ref[...] = jnp.cos(angles)
-        sin_ref[...] = jnp.where(first, -sin, sin)
-
-    cos = cos_ref[...]
-    sin = sin_ref[...]
-
-    def turned(raw, gain):
-        floats = raw.astype(F32)
-        mean = jnp.mean(floats * floats, axis=-1, keepdims=True)
-        normed = floats * lax.rsqrt(mean + EPSILON) * gain
-        other = jnp.where(first, pltpu.roll(normed, 96, 1), pltpu.roll(normed, 32, 1))
-        return (normed * cos + other * sin).astype(BF16)
-
-    key = turned(k_ref[...], kg_ref[...])
+        lane = lax.broadcasted_iota(jnp.int32, (GRID_W, HEAD_DIM), 1)
+        line = lax.broadcasted_iota(jnp.int32, (1, HEAD_DIM), 1)
+        low = lax.bitwise_and(line, 32) == 0
+        start = lax.shift_right_logical(place_ref[0], 3) * (tokens // GRID_W)
+        for which, gain_ref in enumerate((qg_ref, kg_ref)):
+            gain = gain_ref[...]
+            wide = jnp.broadcast_to(gain, (8, HEAD_DIM))
+            other = jnp.where(low, pltpu.roll(wide, 96, 1)[0:1], pltpu.roll(wide, 32, 1)[0:1])
+            for kind, scale in enumerate((gain, other)):
+                for i in range(tokens // GRID_W):
+                    at_row = row_ref[kind, pl.ds(start + i, 1), :]
+                    table = jnp.where(lane < HEAD_DIM // 2, at_row, col_ref[kind])
+                    table_ref[which, kind, i * GRID_W : (i + 1) * GRID_W, :] = table * scale
+
+    ones = jnp.ones((HEAD_DIM, HEAD_DIM), BF16)
+    raw = [q_ref[:, h * HEAD_DIM : (h + 1) * HEAD_DIM] for h in range(group)] + [k_ref[...]]
+    raw = jnp.concatenate(raw, axis=0)
+    floats = raw.astype(F32)
+    square = floats * floats
+    high = square.astype(BF16)
+    low_part = (square - high.astype(F32)).astype(BF16)
+    total = dot(high, ones) + dot(low_part, ones)
+    scale = lax.rsqrt(total * (1.0 / HEAD_DIM) + EPSILON)
+    other = dot(raw, swap_ref[...])
     value = v_ref[...]
-    for h in range(out_ref.shape[0]):
-        query = turned(q_ref[:, h * HEAD_DIM : (h + 1) * HEAD_DIM], qg_ref[...])
-        out_ref[h, :, 0:HEAD_DIM] = query
-        out_ref[h, :, HEAD_DIM : 2 * HEAD_DIM] = key
-        out_ref[h, :, 2 * HEAD_DIM : 3 * HEAD_DIM] = value
+    for h in range(group, -1, -1):
+        rows = slice(h * tokens, (h + 1) * tokens)
+        which = 1 if h == group else 0
+        turned = floats[rows] * table_ref[which, 0] + other[rows] * table_ref[which, 1]
+        turned = (turned * scale[rows]).astype(BF16)
+        if h == group:
+            for g in range(group):
+                out_ref[g, :, HEAD_DIM : 2 * HEAD_DIM] = turned
+                out_ref[g, :, 2 * HEAD_DIM : 3 * HEAD_DIM] = value
+        else:
+            out_ref[h, :, 0:HEAD_DIM] = turned
 
 
 def attend_kernel(x_ref, out_ref, value_ref, even_ref, odd_ref):
@@ -111,7 +138,7 @@
     rank = dot((hit_first + hit_second).astype(BF16), before)
     rank_first = jnp.sum(rank * hit_first, axis=0, keepdims=True).astype(jnp.int32)
     rank_second = jnp.sum(rank * hit_second, axis=0, keepdims=True).astype(jnp.int32)
-    core = place_ref[1]
+    core = lax.bitwise_and(place_ref[0], 1)
 
     def slot_of(expert, rank):
         side = lax.bitwise_xor(lax.bitwise_and(expert, 1), core)
@@ -132,7 +159,11 @@
 
 
 def expert_kernel(y_ref, *rest):
-    *weights, out_ref, wide_ref, x_ref = rest
+    weights, late, (out_ref, wide_ref, x_ref, *held, sems) = list(rest[:4]), rest[4:6], rest[6:]
+    copies = [pltpu.make_async_copy(late[i], held[i], sems.at[i]) for i in range(2)]
+    for copy in copies:
+        copy.start()
+    weights += held
     slots, width = y_ref.shape
     sides = [pl.ds(side, slots // 2, stride=2) for side in range(2)]
     blocks = [slice(c * 128, (c + 1) * 128) for c in range(width // 128)]
@@ -143,8 +174,12 @@
     for side in range(2):
         gate_ref, up_ref, down_ref = weights[3 * side : 3 * side + 3]
         gated = dot(x_ref[side], gate_ref[...])
+        if side == 1:
+            copies[0].wait()
         lifted = dot(x_ref[side], up_ref[...])
         hidden = (gated / (1.0 + jnp.exp(-gated)) * lifted).astype(BF16)
+        if side == 1:
+            copies[1].wait()
         made = dot(hidden, down_ref[...])
         for c, cols in enumerate(blocks):
             wide_ref[c, sides[side], :] = made[:, cols]
@@ -184,16 +219,17 @@
     up_weight,
     down_weight,
 ):
-    sp_count = lax.axis_size("sp")
+    line = ("x", "z")
+    sp_count = lax.axis_size(line)
     tokens, width = query_proj.shape[1:]
     length = tokens * sp_count
     chips = sp_count * lax.axis_size("y")
     experts = 2 * chips
     assert sp_count == HEADS and gate_weight.shape[0] == 1 and lax.axis_size("core") == 2
-    quarter = HEAD_DIM // 4
-    inverse = np.float32(10000.0) ** (-np.arange(quarter, dtype=np.float32) / np.float32(quarter))
-    inverse = jnp.asarray(np.tile(inverse.astype(np.float32), 4)[None])
-    place = jnp.stack([lax.axis_index("sp"), lax.axis_index("core")]).astype(jnp.int32)
+    place = lax.axis_index(("z", "x", "y", "core")).astype(jnp.int32).reshape(1)
+    row_table = jnp.asarray(angle_tables(length // GRID_W))
+    col_table = jnp.asarray(angle_tables(GRID_W))
+    swap_table = jnp.asarray(partner_matrix(), BF16)
     swap = [(0, 1), (1, 0)]
     own = (gate_weight[0], up_weight[0], down_weight[0])
     partner = tuple(lax.ppermute(one, "core", swap) for one in own)
@@ -214,14 +250,26 @@
             pl.BlockSpec((tokens, HEAD_DIM), lambda n: (0, n)),
             fixed(1, HEAD_DIM),
             fixed(1, HEAD_DIM),
-            fixed(1, HEAD_DIM),
+            fixed(*row_table.shape),
+            fixed(*col_table.shape),
+            fixed(*swap_table.shape),
         ],
         out_specs=pl.BlockSpec((group, tokens, 3 * HEAD_DIM), lambda n: (n, 0, 0)),
-        scratch_shapes=[pltpu.VMEM((tokens, HEAD_DIM), F32)] * 2,
+        scratch_shapes=[pltpu.VMEM((2, 2, tokens, HEAD_DIM), F32)],
         compiler_params=limit(63),
         name="pack",
-    )(place, query_proj[0], key_proj[0], value_proj[0], query_gain[None], key_gain[None], inverse)
-    gathered = lax.all_to_all(packed, "sp", 0, 0, tiled=True)
+    )(
+        place,
+        query_proj[0],
+        key_proj[0],
+        value_proj[0],
+        query_gain[None],
+        key_gain[None],
+        row_table,
+        col_table,
+        swap_table,
+    )
+    gathered = lax.all_to_all(packed, line, 0, 0, tiled=True)
     block = 512
     attended = pl.pallas_call(
         attend_kernel,
@@ -241,7 +289,7 @@
         ),
         name="attend",
     )(gathered.reshape(length, 3 * HEAD_DIM))
-    attended = lax.all_to_all(attended.reshape(sp_count, tokens, HEAD_DIM), "sp", 0, 0, tiled=True)
+    attended = lax.all_to_all(attended.reshape(sp_count, tokens, HEAD_DIM), line, 0, 0, tiled=True)
     hbm = pl.BlockSpec(memory_space=pltpu.HBM)
     sent, stream, slots = pl.pallas_call(
         proj_kernel,
@@ -267,17 +315,19 @@
         route_ids[0].T,
         *partner,
     )
-    peers = ("sp", "y")
+    peers = ("z", "x", "y")
     arrived = lax.all_to_all(sent, peers, 0, 0, tiled=True)
     rows = experts * CAP
     answered = pl.pallas_call(
         expert_kernel,
         out_shape=jax.ShapeDtypeStruct((rows, width), BF16),
-        in_specs=[vmem] * 7,
+        in_specs=[vmem] * 5 + [hbm] * 2,
         out_specs=vmem,
         scratch_shapes=[
             pltpu.VMEM((width // 128, rows, 128), F32),
             pltpu.VMEM((2, rows // 2, width), BF16),
+            *[pltpu.VMEM(one.shape, BF16) for one in partner[1:]],
+            pltpu.SemaphoreType.DMA((2,)),
         ],
         compiler_params=limit(24),
         name="expert",
@@ -295,26 +345,26 @@
 
 
 def solution(mesh):
-    assert mesh.axis_names[0] == "sp"
-    grid = mesh.devices.reshape(mesh.devices.shape[0], -1, 2)
-    mesh = Mesh(grid, ("sp", "y", "core"))
+    assert mesh.devices.shape == (16, 8)
+    grid = mesh.devices.reshape(4, 4, 4, 2)
+    mesh = Mesh(grid, ("z", "x", "y", "core"))
     placed = (
-        P(("y", "core"), "sp", None),
-        P(("y", "core"), "sp", None),
-        P(("y", "core"), "sp", None),
-        P(("y", "core"), "sp", None),
-        P(),
-        P(),
-        P(),
-        P(),
-        P(),
-        P(("y", "core"), "sp", None),
-        P(("y", "core"), "sp"),
-        P(("y", "core"), "sp"),
-        P(("sp", "y", "core"), None, None),
-        P(("sp", "y", "core"), None, None),
-        P(("sp", "y", "core"), None, None),
+        P(("y", "core"), ("z", "x"), None),
+        P(("y", "core"), ("z", "x"), None),
+        P(("y", "core"), ("z", "x"), None),
+        P(("y", "core"), ("z", "x"), None),
+        P(),
+        P(),
+        P(),
+        P(),
+        P(),
+        P(("y", "core"), ("z", "x"), None),
+        P(("y", "core"), ("z", "x")),
+        P(("y", "core"), ("z", "x")),
+        P(("z", "x", "y", "core"), None, None),
+        P(("z", "x", "y", "core"), None, None),
+        P(("z", "x", "y", "core"), None, None),
     )
     return jax.shard_map(
-        local, mesh=mesh, in_specs=placed, out_specs=P(("y", "core"), "sp", None), check_vma=False
+        local, mesh=mesh, in_specs=placed, out_specs=P(("y", "core"), ("z", "x"), None), check_vma=False
     )

time: 141 us -> 133 us (0.943)
  blocking collectives: 83.2 us -> 79 us
  Pallas kernels: 23.5 us -> 21.3 us
    all_to_all x1, blocking collectives: 35.8 us -> 33.9 us  [local(): arrived = lax.all_to_all(sent, peers, 0, 0, tiled=True)]
    all_to_all x1, blocking collectives: 33 us -> 31.3 us  [local(): lax.all_to_all(answered.reshape(chips, 2 * CAP, width), peers, 0, 0, tile...]
  transfers between devices with their start and end apart: 4 -> 4, of which waited for: 1 -> 1; matrix products, arithmetic and copies ran while one was open for 0% -> 0% of each run, Pallas kernels for 5% -> 6%
where the time goes in v2:
time: 133 us; the launch traced here: 132 us
  blocking collectives  79 us (59%)
  waiting for transfers between devices  23.2 us (17%)
  Pallas kernels  21.3 us (16%)
  starting transfers between devices  8.72 us (7%)
    all_to_all x1, blocking collectives, local(): arrived = lax.all_to_all(sent, peers, 0, 0, tiled=True)  33.9 us
    all_to_all x1, blocking collectives, local(): lax.all_to_all(answered.reshape(chips, 2 * CAP, width), peers, 0, 0, tile...  31.3 us
    all_to_all x1, waiting for transfers between devices, local(): gathered = lax.all_to_all(packed, line, 0, 0, tiled=True)  23.2 us
    all_to_all x1, blocking collectives, local(): lax.all_to_all(attended.reshape(sp_count, tokens, HEAD_DIM), line, 0, 0,...  13.8 us
    all_to_all x1, starting transfers between devices, local(): gathered = lax.all_to_all(packed, line, 0, 0, tiled=True)  8.04 us
    pallas_call x1, Pallas kernels, local(): pl.pallas_call(attend_kernel, out_shape=jax.ShapeDtypeStruct((length, HEA...  7.43 us
    pallas_call x1, Pallas kernels, local(): pl.pallas_call(expert_kernel, out_shape=jax.ShapeDtypeStruct((rows, width...  5.73 us
    pallas_call x1, Pallas kernels, local(): pl.pallas_call(pack_kernel, grid=(KV_HEADS,), out_shape=jax.ShapeDtypeStr...  4.09 us
  transfers between devices with their start and end apart: 4, of which 1 were waited for; matrix products, arithmetic and copies ran while one was open for 0% of the time, Pallas kernels for 6%

profile of v2, /device:TPU:0, one launch (start us, length us, event | category | flops | bytes accessed | tf_op | source)
XLA Modules:
  0.0 132.4 jit_solution(11240216260487573227)
XLA Ops:
  0.0 4.1 %pack.1 = bf16[16,128,384]{2,1,0:T(8,128)(2,1)} custom-call(s32[1]{0:T(128)} %bitcast.place_ref, bf16[128,2048]{1,0:T(8,128)(2,1)} %bitcast.37, bf16[128,512]{1,0:T(8,128)(2,1)} %bitcast.38, bf16[128,512]{1,0:T(8,128)(2,1)} %bitcast.39, f32[1,128]{1,0:T(1,128)} %bitcast.40, f32[1,128]{1,0:T(1,128)} %bitcast.41, f32[2,32,128]{2,1,0:T(8,128)} %constant.27.clone.row_ref, ...), custom_call_target="tpu_custom_call" | custom-call | tf_op jit(solution)/shard_map/pack/pallas_call | solution.py:242
  4.1 8.0 %all-to-all-start = ((bf16[16,128,384]{2,1,0:T(8,128)(2,1)}), bf16[16,128,384]{2,1,0:T(8,128)(2,1)}, u32[]{:S(2)}, u32[]{:S(2)}) async-start(bf16[16,128,384]{2,1,0:T(8,128)(2,1)} %pack.1), calls=%async_computation | async-start | bytes 3145728 | tf_op jit(solution)/shard_map/all_to_all | solution.py:272
  12.1 0.1 collective-permute-start
  12.2 0.5 collective-permute-start.1
  12.7 0.1 collective-permute-start.2
  12.8 23.2 %all-to-all-done = bf16[16,128,384]{2,1,0:T(8,128)(2,1)} async-done(((bf16[16,128,384]{2,1,0:T(8,128)(2,1)}), bf16[16,128,384]{2,1,0:T(8,128)(2,1)}, u32[]{:S(2)}, u32[]{:S(2)}) %all-to-all-start) | async-done | bytes 1572896 | tf_op jit(solution)/shard_map/all_to_all | solution.py:272
  36.0 0.0 slice-start
  36.0 0.0 slice-start.1
  36.0 0.0 copy-start.3
  36.0 0.0 copy-start.4
  36.0 0.0 copy-start.5
  36.0 0.0 copy-start.6
  36.0 7.4 %attend.1 = bf16[2048,128]{1,0:T(8,128)(2,1)S(1)} custom-call(bf16[2048,384]{1,0:T(8,128)(2,1)} %bitcast.6.x_ref), custom_call_target="tpu_custom_call" | custom-call | flops 8589934592 | bytes 2097152 | tf_op jit(solution)/shard_map/attend/pallas_call | solution.py:274
  43.5 13.8 %all_to_all.20.att_ref = bf16[16,128,128]{2,1,0:T(8,128)(2,1)S(1)} all-to-all(bf16[16,128,128]{2,1,0:T(8,128)(2,1)S(1)} %bitcast.33), channel_id=1, replica_groups=mesh['z'=4,'x'=4,'y'=4,'core'=2] {'x','z'}, dimensions={0} | all-to-all | bytes 1048576 | tf_op jit(solution)/shard_map/all_to_all | solution.py:292
  57.2 0.0 collective-permute-done.rest_0_.rest_3_
  57.2 0.0 collective-permute-done.1.rest_1_.rest_4_
  57.2 0.0 collective-permute-done.2.rest_2_.rest_5_
  57.2 0.0 slice-done
  57.3 0.0 slice-done.1
  57.3 0.0 copy-done.3
  57.3 0.0 copy-done.4
  57.3 0.0 copy-done.5
  57.3 0.0 copy-done.6
  57.3 0.0 copy-start.2
  57.3 2.4 %project.1 = (bf16[64,8,2048]{2,1,0:T(8,128)(2,1)S(1)}, bf16[128,2048]{1,0:T(8,128)(2,1)S(1)}, s32[8,128]{1,0:T(8,128)S(1)}) custom-call(s32[1]{0:T(128)} %bitcast.place_ref, bf16[16,128,128]{2,1,0:T(8,128)(2,1)S(1)} %all_to_all.20.att_ref, bf16[2048,2048]{1,0:T(8,128)(2,1)S(1)} %bitcast.22, bf16[128,2048]{1,0:T(8,128)(2,1)S(1)} %bitcast.32, ...), custom_call_target="tpu_custom_call" | custom-call | tf_op jit(solution)/shard_map/project/pallas_call | solution.py:294
  59.8 0.0 copy-start
  59.8 0.0 copy-start.1
  59.8 33.9 %all_to_all.21 = bf16[64,8,2048]{2,1,0:T(8,128)(2,1)S(1)} all-to-all(bf16[64,8,2048]{2,1,0:T(8,128)(2,1)S(1)} %get-tuple-element.8), channel_id=1, replica_groups=mesh['z'=4,'x'=4,'y'=4,'core'=2] {'z','x','y'}, dimensions={0} | all-to-all | bytes 4194304 | tf_op jit(solution)/shard_map/all_to_all | solution.py:319
  93.7 0.0 copy-done.2
  93.7 0.0 copy-done
  93.7 0.0 copy-done.1
  93.7 5.7 %expert.1 = bf16[512,2048]{1,0:T(8,128)(2,1)S(1)} custom-call(bf16[512,2048]{1,0:T(8,128)(2,1)S(1)} %bitcast.24, bf16[2048,512]{1,0:T(8,128)(2,1)S(1)} %bitcast.27, bf16[2048,512]{1,0:T(8,128)(2,1)S(1)} %bitcast.29, bf16[512,2048]{1,0:T(8,128)(2,1)S(1)} %bitcast.31, bf16[2048,512]{1,0:T(8,128)(2,1)S(1)} %collective-permute-done.rest_0_.rest_3_, ...), custom_call_target="tpu_custom_call" | custom-call | tf_op jit(solution)/shard_map/expert/pallas_call | solution.py:321
  99.5 0.0 copy-start.7
  99.5 0.0 copy-start.8
  99.5 31.3 %all_to_all.22 = bf16[64,8,2048]{2,1,0:T(8,128)(2,1)S(1)} all-to-all(bf16[64,8,2048]{2,1,0:T(8,128)(2,1)S(1)} %bitcast.25), channel_id=1, replica_groups=mesh['z'=4,'x'=4,'y'=4,'core'=2] {'z','x','y'}, dimensions={0} | all-to-all | bytes 4194304 | tf_op jit(solution)/shard_map/all_to_all | solution.py:335
  130.8 0.0 copy-done.7
  130.8 0.0 copy-done.8
  130.8 1.6 %combine.1 = bf16[128,2048]{1,0:T(8,128)(2,1)} custom-call(bf16[512,2048]{1,0:T(8,128)(2,1)S(1)} %bitcast.23, bf16[128,2048]{1,0:T(8,128)(2,1)S(1)} %get-tuple-element.9.stream_ref, s32[8,128]{1,0:T(8,128)S(1)} %get-tuple-element.10.slot_ref, f32[1,128]{1,0:T(1,128)S(1)} %copy-done.7, f32[1,128]{1,0:T(1,128)S(1)} %copy-done.8), custom_call_target="tpu_custom_call" | custom-call | tf_op jit(solution)/shard_map/combine/pallas_call | solution.py:336
  (1 shorter events, 0.0 us)
Async XLA Ops:
  4.1 31.9 %all-to-all-start = ((bf16[16,128,384]{2,1,0:T(8,128)(2,1)}), bf16[16,128,384]{2,1,0:T(8,128)(2,1)}, u32[]{:S(2)}, u32[]{:S(2)}) async-start(bf16[16,128,384]{2,1,0:T(8,128)(2,1)} %pack.1), calls=%async_computation | async-start | bytes 3145728 | tf_op jit(solution)/shard_map/all_to_all | solution.py:272
  12.1 45.1 %collective-permute-start = (bf16[2048,512]{1,0:T(8,128)(2,1)}, bf16[2048,512]{1,0:T(8,128)(2,1)S(1)}, u32[]{:S(2)}, u32[]{:S(2)}) collective-permute-start(bf16[2048,512]{1,0:T(8,128)(2,1)} %bitcast.26), channel_id=1, source_target_pairs={{0,1},{1,0},{2,3},{3,2},{4,5},{5,4},{6,7},{7,6},{8,9},{9,8},{10,11... | collective-permute-start | bytes 6291464 | tf_op jit(solution)/shard_map/ppermute | solution.py:235
  12.2 45.0 %collective-permute-start.1 = (bf16[2048,512]{1,0:T(8,128)(2,1)}, bf16[2048,512]{1,0:T(8,128)(2,1)}, u32[]{:S(2)}, u32[]{:S(2)}) collective-permute-start(bf16[2048,512]{1,0:T(8,128)(2,1)} %bitcast.28), channel_id=1, source_target_pairs={{0,1},{1,0},{2,3},{3,2},{4,5},{5,4},{6,7},{7,6},{8,9},{9,8},{10,11... | collective-permute-start | bytes 6291464 | tf_op jit(solution)/shard_map/ppermute | solution.py:235
  12.7 44.5 %collective-permute-start.2 = (bf16[512,2048]{1,0:T(8,128)(2,1)}, bf16[512,2048]{1,0:T(8,128)(2,1)}, u32[]{:S(2)}, u32[]{:S(2)}) collective-permute-start(bf16[512,2048]{1,0:T(8,128)(2,1)} %bitcast.30), channel_id=1, source_target_pairs={{0,1},{1,0},{2,3},{3,2},{4,5},{5,4},{6,7},{7,6},{8,9},{9,8},{10,11... | collective-permute-start | bytes 6291464 | tf_op jit(solution)/shard_map/ppermute | solution.py:235
  36.0 21.3 %slice-start = ((s8[8388608]{0:T(1024)(128)(4,1)}), s8[4194304]{0:T(1024)(128)(4,1)S(1)}, s32[]{:S(2)}) async-start(s8[8388608]{0:T(1024)(128)(4,1)} %bitcast.21), calls=%async_computation.4 | async-start | bytes 8388608
  36.0 21.3 %slice-start.1 = ((s8[8388608]{0:T(1024)(128)(4,1)}), s8[4194304]{0:T(1024)(128)(4,1)S(1)}, s32[]{:S(2)}) async-start(s8[8388608]{0:T(1024)(128)(4,1)} %bitcast.21), calls=%async_computation.5 | async-start | bytes 8388608
  36.0 21.3 %copy-start.3 = (bf16[1,128,2048]{2,1,0:T(8,128)(2,1)S(1)}, bf16[1,128,2048]{2,1,0:T(8,128)(2,1)}, u32[]{:S(2)}) copy-start(bf16[1,128,2048]{2,1,0:T(8,128)(2,1)} %param.18) | copy-start | bytes 1572868
  36.0 21.3 %copy-start.4 = (f32[2048]{0:T(1024)S(1)}, f32[2048]{0:T(1024)}, u32[]{:S(2)}) copy-start(f32[2048]{0:T(1024)} %param.25) | copy-start | bytes 24580
  36.0 21.3 %copy-start.5 = (f32[2048]{0:T(1024)S(1)}, f32[2048]{0:T(1024)}, u32[]{:S(2)}) copy-start(f32[2048]{0:T(1024)} %param.26) | copy-start | bytes 24580
  36.0 21.3 %copy-start.6 = (s32[1,128,2]{1,2,0:T(2,128)S(1)}, s32[1,128,2]{1,2,0:T(2,128)}, u32[]{:S(2)}) copy-start(s32[1,128,2]{1,2,0:T(2,128)} %param.27) | copy-start | bytes 3076
  57.3 36.4 %copy-start.2 = (bf16[1,512,2048]{2,1,0:T(8,128)(2,1)S(1)}, bf16[1,512,2048]{2,1,0:T(8,128)(2,1)}, u32[]{:S(2)}) copy-start(bf16[1,512,2048]{2,1,0:T(8,128)(2,1)} %param.32) | copy-start | bytes 6291460
  59.8 34.0 %copy-start = (bf16[1,2048,512]{2,1,0:T(8,128)(2,1)S(1)}, bf16[1,2048,512]{2,1,0:T(8,128)(2,1)}, u32[]{:S(2)}) copy-start(bf16[1,2048,512]{2,1,0:T(8,128)(2,1)} %param.30) | copy-start | bytes 6291460
  59.8 34.0 %copy-start.1 = (bf16[1,2048,512]{2,1,0:T(8,128)(2,1)S(1)}, bf16[1,2048,512]{2,1,0:T(8,128)(2,1)}, u32[]{:S(2)}) copy-start(bf16[1,2048,512]{2,1,0:T(8,128)(2,1)} %param.31) | copy-start | bytes 6291460
  99.5 31.3 %copy-start.7 = (f32[1,128]{1,0:T(1,128)S(1)}, f32[1,128]{1,0:T(1,128)}, u32[]{:S(2)}) copy-start(f32[1,128]{1,0:T(1,128)} %weight_ref.1) | copy-start | bytes 1540
  99.5 31.3 %copy-start.8 = (f32[1,128]{1,0:T(1,128)S(1)}, f32[1,128]{1,0:T(1,128)}, u32[]{:S(2)}) copy-start(f32[1,128]{1,0:T(1,128)} %share_ref.1) | copy-start | bytes 1540

commit v3 on v2

--- a/solution.py
+++ b/solution.py
@@ -15,6 +15,8 @@
 GRID_W = 64
 CAP = 4
 EPSILON = 1e-06
+LATE_CORE = 0
+STAGGER_NS = 8000
 F32 = jnp.float32
 BF16 = jnp.bfloat16
 
@@ -44,6 +46,11 @@
 ):
     tokens = k_ref.shape[0]
     group = out_ref.shape[0]
+    late = lax.bitwise_and(place_ref[0], 1) == LATE_CORE
+
+    @pl.when((pl.program_id(0) == 0) & late)
+    def _():
+        pl.delay(STAGGER_NS)
 
     @pl.when(pl.program_id(0) == 0)
     def _():
@@ -283,7 +290,7 @@
         ],
         compiler_params=limit(24),
         cost_estimate=pl.CostEstimate(
-            flops=4 * length * length * HEAD_DIM * 4,
+            flops=length * length * HEAD_DIM,
             bytes_accessed=length * HEAD_DIM * 8,
             transcendentals=length * length,
         ),

time: 133 us -> 119 us (0.89)
  waiting for transfers between devices: 23.2 us -> 0.01 us
  blocking collectives: 79 us -> 89 us
  starting transfers between devices: 8.72 us -> 0.51 us
  Pallas kernels: 21.3 us -> 29 us
    all_to_all x0 -> x1, blocking collectives: none -> 23.7 us  [local(): gathered = lax.all_to_all(packed, line, 0, 0, tiled=True)]
    all_to_all x1 -> x0, waiting for transfers between devices: 23.2 us -> none  [local(): gathered = lax.all_to_all(packed, line, 0, 0, tiled=True)]
    all_to_all x1 -> x0, starting transfers between devices: 8.04 us -> none  [local(): gathered = lax.all_to_all(packed, line, 0, 0, tiled=True)]
    pallas_call x1, Pallas kernels: 4.09 us -> 12.1 us  [local(): pl.pallas_call(pack_kernel, grid=(KV_HEADS,), out_shape=jax.ShapeDtypeStr...]
    all_to_all x1, blocking collectives: 33.9 us -> 27 us  [local(): arrived = lax.all_to_all(sent, peers, 0, 0, tiled=True)]
    all_to_all x1, blocking collectives: 31.3 us -> 25 us  [local(): lax.all_to_all(answered.reshape(chips, 2 * CAP, width), peers, 0, 0, tile...]
  transfers between devices with their start and end apart: 4 -> 3, of which waited for: 1 -> 0; matrix products, arithmetic and copies ran while one was open for 0% -> 0% of each run, Pallas kernels for 6% -> 15%
where the time goes in v3:
time: 119 us
  blocking collectives  89 us (75%)
  Pallas kernels  29 us (24%)
    all_to_all x1, blocking collectives, local(): arrived = lax.all_to_all(sent, peers, 0, 0, tiled=True)  27 us
    all_to_all x1, blocking collectives, local(): lax.all_to_all(answered.reshape(chips, 2 * CAP, width), peers, 0, 0, tile...  25 us
    all_to_all x1, blocking collectives, local(): gathered = lax.all_to_all(packed, line, 0, 0, tiled=True)  23.7 us
    all_to_all x1, blocking collectives, local(): lax.all_to_all(attended.reshape(sp_count, tokens, HEAD_DIM), line, 0, 0,...  13.3 us
    pallas_call x1, Pallas kernels, local(): pl.pallas_call(pack_kernel, grid=(KV_HEADS,), out_shape=jax.ShapeDtypeStr...  12.1 us
    pallas_call x1, Pallas kernels, local(): pl.pallas_call(expert_kernel, out_shape=jax.ShapeDtypeStruct((rows, width...  6.78 us
    pallas_call x1, Pallas kernels, local(): pl.pallas_call(attend_kernel, out_shape=jax.ShapeDtypeStruct((length, HEA...  6.11 us
    pallas_call x1, Pallas kernels, local(): pl.pallas_call(proj_kernel, out_shape=(jax.ShapeDtypeStruct((chips, 2 * C...  2.41 us
  transfers between devices with their start and end apart: 3, of which 0 were waited for; matrix products, arithmetic and copies ran while one was open for 0% of the time, Pallas kernels for 15%

profile of v3, /device:TPU:0, one launch (start us, length us, event | category | flops | bytes accessed | tf_op | source)
XLA Modules:
  0.0 118.7 jit_solution(12601492969500700265)
XLA Ops:
  0.0 0.0 collective-permute-start
  0.0 0.5 collective-permute-start.1
  0.5 0.0 collective-permute-start.2
  0.5 12.1 %pack.1 = bf16[16,128,384]{2,1,0:T(8,128)(2,1)} custom-call(s32[1]{0:T(128)} %bitcast.place_ref, bf16[128,2048]{1,0:T(8,128)(2,1)} %bitcast.36, bf16[128,512]{1,0:T(8,128)(2,1)} %bitcast.37, bf16[128,512]{1,0:T(8,128)(2,1)} %bitcast.38, f32[1,128]{1,0:T(1,128)} %bitcast.39, f32[1,128]{1,0:T(1,128)} %bitcast.40, f32[2,32,128]{2,1,0:T(8,128)} %constant.27.clone.row_ref, ...), custom_call_target="tpu_custom_call" | custom-call | tf_op jit(solution)/shard_map/pack/pallas_call | solution.py:249
  12.6 23.7 %all_to_all.20 = bf16[16,128,384]{2,1,0:T(8,128)(2,1)S(1)} all-to-all(bf16[16,128,384]{2,1,0:T(8,128)(2,1)} %pack.1), channel_id=1, replica_groups=mesh['z'=4,'x'=4,'y'=4,'core'=2] {'x','z'}, dimensions={0} | all-to-all | bytes 3145728 | tf_op jit(solution)/shard_map/all_to_all | solution.py:279
  36.3 0.0 copy-start
  36.3 0.0 copy-start.4
  36.4 0.0 copy-start.5
  36.4 0.0 copy-start.6
  36.4 0.0 copy-start.7
  36.4 6.1 %attend.1 = bf16[2048,128]{1,0:T(8,128)(2,1)S(1)} custom-call(bf16[2048,384]{1,0:T(8,128)(2,1)S(1)} %bitcast.30), custom_call_target="tpu_custom_call" | custom-call | flops 536870912 | bytes 2097152 | tf_op jit(solution)/shard_map/attend/pallas_call | solution.py:281
  42.5 13.3 %all_to_all.21.att_ref = bf16[16,128,128]{2,1,0:T(8,128)(2,1)S(1)} all-to-all(bf16[16,128,128]{2,1,0:T(8,128)(2,1)S(1)} %bitcast.32), channel_id=1, replica_groups=mesh['z'=4,'x'=4,'y'=4,'core'=2] {'x','z'}, dimensions={0} | all-to-all | bytes 1048576 | tf_op jit(solution)/shard_map/all_to_all | solution.py:299
  55.8 0.0 collective-permute-done.rest_0_.rest_3_
  55.8 0.0 collective-permute-done.1.rest_1_.rest_4_
  55.8 0.0 collective-permute-done.2.rest_2_.rest_5_
  55.8 0.0 copy-done
  55.9 0.0 copy-done.4
  55.9 0.0 copy-done.5
  55.9 0.0 copy-done.6
  55.9 0.0 copy-done.7
  55.9 0.0 copy-start.3
  55.9 2.4 %project.1 = (bf16[64,8,2048]{2,1,0:T(8,128)(2,1)S(1)}, bf16[128,2048]{1,0:T(8,128)(2,1)S(1)}, s32[8,128]{1,0:T(8,128)S(1)}) custom-call(s32[1]{0:T(128)} %bitcast.place_ref, bf16[16,128,128]{2,1,0:T(8,128)(2,1)S(1)} %all_to_all.21.att_ref, bf16[2048,2048]{1,0:T(8,128)(2,1)S(1)} %copy-done, bf16[128,2048]{1,0:T(8,128)(2,1)S(1)} %bitcast.31, ...), custom_call_target="tpu_custom_call" | custom-call | tf_op jit(solution)/shard_map/project/pallas_call | solution.py:301
  58.3 0.0 copy-start.1
  58.3 0.0 copy-start.2
  58.4 27.0 %all_to_all.22 = bf16[64,8,2048]{2,1,0:T(8,128)(2,1)S(1)} all-to-all(bf16[64,8,2048]{2,1,0:T(8,128)(2,1)S(1)} %get-tuple-element.8), channel_id=1, replica_groups=mesh['z'=4,'x'=4,'y'=4,'core'=2] {'z','x','y'}, dimensions={0} | all-to-all | bytes 4194304 | tf_op jit(solution)/shard_map/all_to_all | solution.py:326
  85.3 0.0 copy-done.3
  85.3 0.0 copy-done.1
  85.3 0.0 copy-done.2
  85.3 6.8 %expert.1 = bf16[512,2048]{1,0:T(8,128)(2,1)S(1)} custom-call(bf16[512,2048]{1,0:T(8,128)(2,1)S(1)} %bitcast.22, bf16[2048,512]{1,0:T(8,128)(2,1)S(1)} %bitcast.25, bf16[2048,512]{1,0:T(8,128)(2,1)S(1)} %bitcast.27, bf16[512,2048]{1,0:T(8,128)(2,1)S(1)} %bitcast.29, bf16[2048,512]{1,0:T(8,128)(2,1)} %collective-permute-done.rest_0_.rest_3_, ...), custom_call_target="tpu_custom_call" | custom-call | tf_op jit(solution)/shard_map/expert/pallas_call | solution.py:328
  92.1 0.0 copy-start.8
  92.1 0.0 copy-start.9
  92.1 25.0 %all_to_all.23 = bf16[64,8,2048]{2,1,0:T(8,128)(2,1)S(1)} all-to-all(bf16[64,8,2048]{2,1,0:T(8,128)(2,1)S(1)} %bitcast.23), channel_id=1, replica_groups=mesh['z'=4,'x'=4,'y'=4,'core'=2] {'z','x','y'}, dimensions={0} | all-to-all | bytes 4194304 | tf_op jit(solution)/shard_map/all_to_all | solution.py:342
  117.1 0.0 copy-done.8
  117.1 0.0 copy-done.9
  117.1 1.6 %combine.1 = bf16[128,2048]{1,0:T(8,128)(2,1)} custom-call(bf16[512,2048]{1,0:T(8,128)(2,1)S(1)} %bitcast.21, bf16[128,2048]{1,0:T(8,128)(2,1)S(1)} %get-tuple-element.9.stream_ref, s32[8,128]{1,0:T(8,128)S(1)} %get-tuple-element.10.slot_ref, f32[1,128]{1,0:T(1,128)S(1)} %copy-done.8, f32[1,128]{1,0:T(1,128)S(1)} %copy-done.9), custom_call_target="tpu_custom_call" | custom-call | tf_op jit(solution)/shard_map/combine/pallas_call | solution.py:343
Async XLA Ops:
  0.0 55.8 %collective-permute-start = (bf16[2048,512]{1,0:T(8,128)(2,1)}, bf16[2048,512]{1,0:T(8,128)(2,1)}, u32[]{:S(2)}, u32[]{:S(2)}) collective-permute-start(bf16[2048,512]{1,0:T(8,128)(2,1)} %bitcast.24), channel_id=1, source_target_pairs={{0,1},{1,0},{2,3},{3,2},{4,5},{5,4},{6,7},{7,6},{8,9},{9,8},{10,11... | collective-permute-start | bytes 6291464 | tf_op jit(solution)/shard_map/ppermute | solution.py:242
  0.0 55.8 %collective-permute-start.1 = (bf16[2048,512]{1,0:T(8,128)(2,1)}, bf16[2048,512]{1,0:T(8,128)(2,1)}, u32[]{:S(2)}, u32[]{:S(2)}) collective-permute-start(bf16[2048,512]{1,0:T(8,128)(2,1)} %bitcast.26), channel_id=1, source_target_pairs={{0,1},{1,0},{2,3},{3,2},{4,5},{5,4},{6,7},{7,6},{8,9},{9,8},{10,11... | collective-permute-start | bytes 6291464 | tf_op jit(solution)/shard_map/ppermute | solution.py:242
  0.5 55.3 %collective-permute-start.2 = (bf16[512,2048]{1,0:T(8,128)(2,1)}, bf16[512,2048]{1,0:T(8,128)(2,1)}, u32[]{:S(2)}, u32[]{:S(2)}) collective-permute-start(bf16[512,2048]{1,0:T(8,128)(2,1)} %bitcast.28), channel_id=1, source_target_pairs={{0,1},{1,0},{2,3},{3,2},{4,5},{5,4},{6,7},{7,6},{8,9},{9,8},{10,11... | collective-permute-start | bytes 6291464 | tf_op jit(solution)/shard_map/ppermute | solution.py:242
  36.3 19.5 %copy-start = (bf16[2048,2048]{1,0:T(8,128)(2,1)S(1)}, bf16[2048,2048]{1,0:T(8,128)(2,1)}, u32[]{:S(2)}) copy-start(bf16[2048,2048]{1,0:T(8,128)(2,1)} %w_ref.1) | copy-start | bytes 25165828
  36.3 19.5 %copy-start.4 = (bf16[1,128,2048]{2,1,0:T(8,128)(2,1)S(1)}, bf16[1,128,2048]{2,1,0:T(8,128)(2,1)}, u32[]{:S(2)}) copy-start(bf16[1,128,2048]{2,1,0:T(8,128)(2,1)} %param.18) | copy-start | bytes 1572868
  36.4 19.5 %copy-start.5 = (f32[2048]{0:T(1024)S(1)}, f32[2048]{0:T(1024)}, u32[]{:S(2)}) copy-start(f32[2048]{0:T(1024)} %param.25) | copy-start | bytes 24580
  36.4 19.5 %copy-start.6 = (f32[2048]{0:T(1024)S(1)}, f32[2048]{0:T(1024)}, u32[]{:S(2)}) copy-start(f32[2048]{0:T(1024)} %param.26) | copy-start | bytes 24580
  36.4 19.5 %copy-start.7 = (s32[1,128,2]{1,2,0:T(2,128)S(1)}, s32[1,128,2]{1,2,0:T(2,128)}, u32[]{:S(2)}) copy-start(s32[1,128,2]{1,2,0:T(2,128)} %param.27) | copy-start | bytes 3076
  55.9 29.4 %copy-start.3 = (bf16[1,512,2048]{2,1,0:T(8,128)(2,1)S(1)}, bf16[1,512,2048]{2,1,0:T(8,128)(2,1)}, u32[]{:S(2)}) copy-start(bf16[1,512,2048]{2,1,0:T(8,128)(2,1)} %param.32) | copy-start | bytes 6291460
  58.3 27.0 %copy-start.1 = (bf16[1,2048,512]{2,1,0:T(8,128)(2,1)S(1)}, bf16[1,2048,512]{2,1,0:T(8,128)(2,1)}, u32[]{:S(2)}) copy-start(bf16[1,2048,512]{2,1,0:T(8,128)(2,1)} %param.30) | copy-start | bytes 6291460
  58.3 27.0 %copy-start.2 = (bf16[1,2048,512]{2,1,0:T(8,128)(2,1)S(1)}, bf16[1,2048,512]{2,1,0:T(8,128)(2,1)}, u32[]{:S(2)}) copy-start(bf16[1,2048,512]{2,1,0:T(8,128)(2,1)} %param.31) | copy-start | bytes 6291460
  92.1 25.0 %copy-start.8 = (f32[1,128]{1,0:T(1,128)S(1)}, f32[1,128]{1,0:T(1,128)}, u32[]{:S(2)}) copy-start(f32[1,128]{1,0:T(1,128)} %weight_ref.1) | copy-start | bytes 1540
  92.1 25.0 %copy-start.9 = (f32[1,128]{1,0:T(1,128)S(1)}, f32[1,128]{1,0:T(1,128)}, u32[]{:S(2)}) copy-start(f32[1,128]{1,0:T(1,128)} %share_ref.1) | copy-start | bytes 1540

commit v4 on v3

--- a/solution.py
+++ b/solution.py
@@ -16,7 +16,8 @@
 CAP = 4
 EPSILON = 1e-06
 LATE_CORE = 0
-STAGGER_NS = 8000
+PACK_STEPS = 2
+STAGGER_NS = 8200
 F32 = jnp.float32
 BF16 = jnp.bfloat16
 
@@ -45,7 +46,6 @@
     place_ref, q_ref, k_ref, v_ref, qg_ref, kg_ref, row_ref, col_ref, swap_ref, out_ref, table_ref
 ):
     tokens = k_ref.shape[0]
-    group = out_ref.shape[0]
     late = lax.bitwise_and(place_ref[0], 1) == LATE_CORE
 
     @pl.when((pl.program_id(0) == 0) & late)
@@ -69,7 +69,10 @@
                     table_ref[which, kind, i * GRID_W : (i + 1) * GRID_W, :] = table * scale
 
     ones = jnp.ones((HEAD_DIM, HEAD_DIM), BF16)
-    raw = [q_ref[:, h * HEAD_DIM : (h + 1) * HEAD_DIM] for h in range(group)] + [k_ref[...]]
+    keys = k_ref.shape[1] // HEAD_DIM
+    group = HEADS // KV_HEADS
+    head = lambda ref, h: ref[:, h * HEAD_DIM : (h + 1) * HEAD_DIM]
+    raw = [head(q_ref, h) for h in range(keys * group)] + [head(k_ref, kv) for kv in range(keys)]
     raw = jnp.concatenate(raw, axis=0)
     floats = raw.astype(F32)
     square = floats * floats
@@ -78,18 +81,18 @@
     total = dot(high, ones) + dot(low_part, ones)
     scale = lax.rsqrt(total * (1.0 / HEAD_DIM) + EPSILON)
     other = dot(raw, swap_ref[...])
-    value = v_ref[...]
-    for h in range(group, -1, -1):
+    for h in range(keys * (group + 1)):
         rows = slice(h * tokens, (h + 1) * tokens)
-        which = 1 if h == group else 0
+        which = 1 if h >= keys * group else 0
         turned = floats[rows] * table_ref[which, 0] + other[rows] * table_ref[which, 1]
         turned = (turned * scale[rows]).astype(BF16)
-        if h == group:
-            for g in range(group):
-                out_ref[g, :, HEAD_DIM : 2 * HEAD_DIM] = turned
-                out_ref[g, :, 2 * HEAD_DIM : 3 * HEAD_DIM] = value
-        else:
+        if which == 0:
             out_ref[h, :, 0:HEAD_DIM] = turned
+            continue
+        kv = h - keys * group
+        for g in range(kv * group, (kv + 1) * group):
+            out_ref[g, :, HEAD_DIM : 2 * HEAD_DIM] = turned
+            out_ref[g, :, 2 * HEAD_DIM : 3 * HEAD_DIM] = head(v_ref, kv)
 
 
 def attend_kernel(x_ref, out_ref, value_ref, even_ref, odd_ref):
@@ -166,8 +169,8 @@
 
 
 def expert_kernel(y_ref, *rest):
-    weights, late, (out_ref, wide_ref, x_ref, *held, sems) = list(rest[:4]), rest[4:6], rest[6:]
-    copies = [pltpu.make_async_copy(late[i], held[i], sems.at[i]) for i in range(2)]
+    weights, late, (out_ref, wide_ref, x_ref, *held, sems) = list(rest[:3]), rest[3:6], rest[6:]
+    copies = [pltpu.make_async_copy(late[i], held[i], sems.at[i]) for i in range(3)]
     for copy in copies:
         copy.start()
     weights += held
@@ -180,13 +183,15 @@
             x_ref[side, :, cols] = wide_ref[c, sides[side], :].astype(BF16)
     for side in range(2):
         gate_ref, up_ref, down_ref = weights[3 * side : 3 * side + 3]
+        if side == 1:
+            copies[0].wait()
         gated = dot(x_ref[side], gate_ref[...])
         if side == 1:
-            copies[0].wait()
+            copies[1].wait()
         lifted = dot(x_ref[side], up_ref[...])
         hidden = (gated / (1.0 + jnp.exp(-gated)) * lifted).astype(BF16)
         if side == 1:
-            copies[1].wait()
+            copies[2].wait()
         made = dot(hidden, down_ref[...])
         for c, cols in enumerate(blocks):
             wide_ref[c, sides[side], :] = made[:, cols]
@@ -244,24 +249,24 @@
     vmem = pl.BlockSpec(memory_space=pltpu.VMEM)
     smem = pl.BlockSpec(memory_space=pltpu.SMEM)
     limit = lambda mib: pltpu.CompilerParams(vmem_limit_bytes=mib * 2**20)
-    group = HEADS // KV_HEADS
+    kv_width = key_proj.shape[2]
     fixed = lambda *shape: pl.BlockSpec(shape, lambda n: (0,) * len(shape))
     packed = pl.pallas_call(
         pack_kernel,
-        grid=(KV_HEADS,),
+        grid=(PACK_STEPS,),
         out_shape=jax.ShapeDtypeStruct((HEADS, tokens, 3 * HEAD_DIM), BF16),
         in_specs=[
             smem,
-            pl.BlockSpec((tokens, group * HEAD_DIM), lambda n: (0, n)),
-            pl.BlockSpec((tokens, HEAD_DIM), lambda n: (0, n)),
-            pl.BlockSpec((tokens, HEAD_DIM), lambda n: (0, n)),
+            pl.BlockSpec((tokens, width // PACK_STEPS), lambda n: (0, n)),
+            pl.BlockSpec((tokens, kv_width // PACK_STEPS), lambda n: (0, n)),
+            pl.BlockSpec((tokens, kv_width // PACK_STEPS), lambda n: (0, n)),
             fixed(1, HEAD_DIM),
             fixed(1, HEAD_DIM),
             fixed(*row_table.shape),
             fixed(*col_table.shape),
             fixed(*swap_table.shape),
         ],
-        out_specs=pl.BlockSpec((group, tokens, 3 * HEAD_DIM), lambda n: (n, 0, 0)),
+        out_specs=pl.BlockSpec((HEADS // PACK_STEPS, tokens, 3 * HEAD_DIM), lambda n: (n, 0, 0)),
         scratch_shapes=[pltpu.VMEM((2, 2, tokens, HEAD_DIM), F32)],
         compiler_params=limit(63),
         name="pack",
@@ -328,13 +333,13 @@
     answered = pl.pallas_call(
         expert_kernel,
         out_shape=jax.ShapeDtypeStruct((rows, width), BF16),
-        in_specs=[vmem] * 5 + [hbm] * 2,
+        in_specs=[vmem] * 4 + [hbm] * 3,
         out_specs=vmem,
         scratch_shapes=[
             pltpu.VMEM((width // 128, rows, 128), F32),
             pltpu.VMEM((2, rows // 2, width), BF16),
-            *[pltpu.VMEM(one.shape, BF16) for one in partner[1:]],
-            pltpu.SemaphoreType.DMA((2,)),
+            *[pltpu.VMEM(one.shape, BF16) for one in partner],
+            pltpu.SemaphoreType.DMA((3,)),
         ],
         compiler_params=limit(24),
         name="expert",

time: 119 us -> 117 us (0.983)
  Pallas kernels: 29 us -> 27.4 us
where the time goes in v4:
time: 117 us
  blocking collectives  89 us (76%)
  Pallas kernels  27.4 us (23%)
    all_to_all x1, blocking collectives, local(): arrived = lax.all_to_all(sent, peers, 0, 0, tiled=True)  26.9 us
    all_to_all x1, blocking collectives, local(): lax.all_to_all(answered.reshape(chips, 2 * CAP, width), peers, 0, 0, tile...  25.1 us
    all_to_all x1, blocking collectives, local(): gathered = lax.all_to_all(packed, line, 0, 0, tiled=True)  23.7 us
    all_to_all x1, blocking collectives, local(): lax.all_to_all(attended.reshape(sp_count, tokens, HEAD_DIM), line, 0, 0,...  13.3 us
    pallas_call x1, Pallas kernels, local(): pl.pallas_call(pack_kernel, grid=(PACK_STEPS,), out_shape=jax.ShapeDtypeS...  11.2 us
    pallas_call x1, Pallas kernels, local(): pl.pallas_call(attend_kernel, out_shape=jax.ShapeDtypeStruct((length, HEA...  6.11 us
    pallas_call x1, Pallas kernels, local(): pl.pallas_call(expert_kernel, out_shape=jax.ShapeDtypeStruct((rows, width...  6.09 us
    pallas_call x1, Pallas kernels, local(): pl.pallas_call(proj_kernel, out_shape=(jax.ShapeDtypeStruct((chips, 2 * C...  2.42 us
  transfers between devices with their start and end apart: 3, of which 0 were waited for; matrix products, arithmetic and copies ran while one was open for 0% of the time, Pallas kernels for 15%

profile of v4, /device:TPU:0, one launch (start us, length us, event | category | flops | bytes accessed | tf_op | source)
XLA Modules:
  0.0 117.1 jit_solution(7771843643367331559)
XLA Ops:
  0.0 0.0 collective-permute-start
  0.0 0.5 collective-permute-start.1
  0.5 0.0 collective-permute-start.2
  0.5 11.2 %pack.1 = bf16[16,128,384]{2,1,0:T(8,128)(2,1)} custom-call(s32[1]{0:T(128)} %bitcast.place_ref, bf16[128,2048]{1,0:T(8,128)(2,1)} %bitcast.36, bf16[128,512]{1,0:T(8,128)(2,1)} %bitcast.37, bf16[128,512]{1,0:T(8,128)(2,1)} %bitcast.38, f32[1,128]{1,0:T(1,128)} %bitcast.39, f32[1,128]{1,0:T(1,128)} %bitcast.40, f32[2,32,128]{2,1,0:T(8,128)} %constant.27.clone.row_ref, ...), custom_call_target="tpu_custom_call" | custom-call | tf_op jit(solution)/shard_map/pack/pallas_call | solution.py:254
  11.7 23.7 %all_to_all.20 = bf16[16,128,384]{2,1,0:T(8,128)(2,1)S(1)} all-to-all(bf16[16,128,384]{2,1,0:T(8,128)(2,1)} %pack.1), channel_id=1, replica_groups=mesh['z'=4,'x'=4,'y'=4,'core'=2] {'x','z'}, dimensions={0} | all-to-all | bytes 3145728 | tf_op jit(solution)/shard_map/all_to_all | solution.py:284
  35.4 0.0 copy-start
  35.4 0.0 copy-start.4
  35.4 0.0 copy-start.5
  35.4 0.0 copy-start.6
  35.4 0.0 copy-start.7
  35.4 6.1 %attend.1 = bf16[2048,128]{1,0:T(8,128)(2,1)S(1)} custom-call(bf16[2048,384]{1,0:T(8,128)(2,1)S(1)} %bitcast.30), custom_call_target="tpu_custom_call" | custom-call | flops 536870912 | bytes 2097152 | tf_op jit(solution)/shard_map/attend/pallas_call | solution.py:286
  41.6 13.3 %all_to_all.21.att_ref = bf16[16,128,128]{2,1,0:T(8,128)(2,1)S(1)} all-to-all(bf16[16,128,128]{2,1,0:T(8,128)(2,1)S(1)} %bitcast.32), channel_id=1, replica_groups=mesh['z'=4,'x'=4,'y'=4,'core'=2] {'x','z'}, dimensions={0} | all-to-all | bytes 1048576 | tf_op jit(solution)/shard_map/all_to_all | solution.py:304
  54.9 0.0 collective-permute-done.rest_0_.rest_3_
  54.9 0.0 collective-permute-done.1.rest_1_.rest_4_
  54.9 0.0 collective-permute-done.2.rest_2_.rest_5_
  54.9 0.0 copy-done
  54.9 0.0 copy-done.4
  54.9 0.0 copy-done.5
  54.9 0.0 copy-done.6
  55.0 0.0 copy-done.7
  55.0 0.0 copy-start.3
  55.0 2.4 %project.1 = (bf16[64,8,2048]{2,1,0:T(8,128)(2,1)S(1)}, bf16[128,2048]{1,0:T(8,128)(2,1)S(1)}, s32[8,128]{1,0:T(8,128)S(1)}) custom-call(s32[1]{0:T(128)} %bitcast.place_ref, bf16[16,128,128]{2,1,0:T(8,128)(2,1)S(1)} %all_to_all.21.att_ref, bf16[2048,2048]{1,0:T(8,128)(2,1)S(1)} %copy-done, bf16[128,2048]{1,0:T(8,128)(2,1)S(1)} %bitcast.31, ...), custom_call_target="tpu_custom_call" | custom-call | tf_op jit(solution)/shard_map/project/pallas_call | solution.py:306
  57.4 0.0 copy-start.1
  57.4 0.0 copy-start.2
  57.4 26.9 %all_to_all.22 = bf16[64,8,2048]{2,1,0:T(8,128)(2,1)S(1)} all-to-all(bf16[64,8,2048]{2,1,0:T(8,128)(2,1)S(1)} %get-tuple-element.8), channel_id=1, replica_groups=mesh['z'=4,'x'=4,'y'=4,'core'=2] {'z','x','y'}, dimensions={0} | all-to-all | bytes 4194304 | tf_op jit(solution)/shard_map/all_to_all | solution.py:331
  84.3 0.0 copy-done.3
  84.3 0.0 copy-done.1
  84.3 0.0 copy-done.2
  84.3 6.1 %expert.1 = bf16[512,2048]{1,0:T(8,128)(2,1)S(1)} custom-call(bf16[512,2048]{1,0:T(8,128)(2,1)S(1)} %bitcast.22, bf16[2048,512]{1,0:T(8,128)(2,1)S(1)} %bitcast.25, bf16[2048,512]{1,0:T(8,128)(2,1)S(1)} %bitcast.27, bf16[512,2048]{1,0:T(8,128)(2,1)S(1)} %bitcast.29, bf16[2048,512]{1,0:T(8,128)(2,1)} %collective-permute-done.rest_0_.rest_3_, ...), custom_call_target="tpu_custom_call" | custom-call | tf_op jit(solution)/shard_map/expert/pallas_call | solution.py:333
  90.4 0.0 copy-start.8
  90.4 0.0 copy-start.9
  90.5 25.1 %all_to_all.23 = bf16[64,8,2048]{2,1,0:T(8,128)(2,1)S(1)} all-to-all(bf16[64,8,2048]{2,1,0:T(8,128)(2,1)S(1)} %bitcast.23), channel_id=1, replica_groups=mesh['z'=4,'x'=4,'y'=4,'core'=2] {'z','x','y'}, dimensions={0} | all-to-all | bytes 4194304 | tf_op jit(solution)/shard_map/all_to_all | solution.py:347
  115.5 0.0 copy-done.8
  115.5 0.0 copy-done.9
  115.5 1.6 %combine.1 = bf16[128,2048]{1,0:T(8,128)(2,1)} custom-call(bf16[512,2048]{1,0:T(8,128)(2,1)S(1)} %bitcast.21, bf16[128,2048]{1,0:T(8,128)(2,1)S(1)} %get-tuple-element.9.stream_ref, s32[8,128]{1,0:T(8,128)S(1)} %get-tuple-element.10.slot_ref, f32[1,128]{1,0:T(1,128)S(1)} %copy-done.8, f32[1,128]{1,0:T(1,128)S(1)} %copy-done.9), custom_call_target="tpu_custom_call" | custom-call | tf_op jit(solution)/shard_map/combine/pallas_call | solution.py:348
Async XLA Ops:
  0.0 54.9 %collective-permute-start = (bf16[2048,512]{1,0:T(8,128)(2,1)}, bf16[2048,512]{1,0:T(8,128)(2,1)}, u32[]{:S(2)}, u32[]{:S(2)}) collective-permute-start(bf16[2048,512]{1,0:T(8,128)(2,1)} %bitcast.24), channel_id=1, source_target_pairs={{0,1},{1,0},{2,3},{3,2},{4,5},{5,4},{6,7},{7,6},{8,9},{9,8},{10,11... | collective-permute-start | bytes 6291464 | tf_op jit(solution)/shard_map/ppermute | solution.py:247
  0.0 54.9 %collective-permute-start.1 = (bf16[2048,512]{1,0:T(8,128)(2,1)}, bf16[2048,512]{1,0:T(8,128)(2,1)}, u32[]{:S(2)}, u32[]{:S(2)}) collective-permute-start(bf16[2048,512]{1,0:T(8,128)(2,1)} %bitcast.26), channel_id=1, source_target_pairs={{0,1},{1,0},{2,3},{3,2},{4,5},{5,4},{6,7},{7,6},{8,9},{9,8},{10,11... | collective-permute-start | bytes 6291464 | tf_op jit(solution)/shard_map/ppermute | solution.py:247
  0.5 54.4 %collective-permute-start.2 = (bf16[512,2048]{1,0:T(8,128)(2,1)}, bf16[512,2048]{1,0:T(8,128)(2,1)}, u32[]{:S(2)}, u32[]{:S(2)}) collective-permute-start(bf16[512,2048]{1,0:T(8,128)(2,1)} %bitcast.28), channel_id=1, source_target_pairs={{0,1},{1,0},{2,3},{3,2},{4,5},{5,4},{6,7},{7,6},{8,9},{9,8},{10,11... | collective-permute-start | bytes 6291464 | tf_op jit(solution)/shard_map/ppermute | solution.py:247
  35.4 19.5 %copy-start = (bf16[2048,2048]{1,0:T(8,128)(2,1)S(1)}, bf16[2048,2048]{1,0:T(8,128)(2,1)}, u32[]{:S(2)}) copy-start(bf16[2048,2048]{1,0:T(8,128)(2,1)} %w_ref.1) | copy-start | bytes 25165828
  35.4 19.5 %copy-start.4 = (bf16[1,128,2048]{2,1,0:T(8,128)(2,1)S(1)}, bf16[1,128,2048]{2,1,0:T(8,128)(2,1)}, u32[]{:S(2)}) copy-start(bf16[1,128,2048]{2,1,0:T(8,128)(2,1)} %param.18) | copy-start | bytes 1572868
  35.4 19.5 %copy-start.5 = (f32[2048]{0:T(1024)S(1)}, f32[2048]{0:T(1024)}, u32[]{:S(2)}) copy-start(f32[2048]{0:T(1024)} %param.25) | copy-start | bytes 24580
  35.4 19.5 %copy-start.6 = (f32[2048]{0:T(1024)S(1)}, f32[2048]{0:T(1024)}, u32[]{:S(2)}) copy-start(f32[2048]{0:T(1024)} %param.26) | copy-start | bytes 24580
  35.4 19.5 %copy-start.7 = (s32[1,128,2]{1,2,0:T(2,128)S(1)}, s32[1,128,2]{1,2,0:T(2,128)}, u32[]{:S(2)}) copy-start(s32[1,128,2]{1,2,0:T(2,128)} %param.27) | copy-start | bytes 3076
  55.0 29.4 %copy-start.3 = (bf16[1,512,2048]{2,1,0:T(8,128)(2,1)S(1)}, bf16[1,512,2048]{2,1,0:T(8,128)(2,1)}, u32[]{:S(2)}) copy-start(bf16[1,512,2048]{2,1,0:T(8,128)(2,1)} %param.32) | copy-start | bytes 6291460
  57.4 26.9 %copy-start.1 = (bf16[1,2048,512]{2,1,0:T(8,128)(2,1)S(1)}, bf16[1,2048,512]{2,1,0:T(8,128)(2,1)}, u32[]{:S(2)}) copy-start(bf16[1,2048,512]{2,1,0:T(8,128)(2,1)} %param.30) | copy-start | bytes 6291460
  57.4 26.9 %copy-start.2 = (bf16[1,2048,512]{2,1,0:T(8,128)(2,1)S(1)}, bf16[1,2048,512]{2,1,0:T(8,128)(2,1)}, u32[]{:S(2)}) copy-start(bf16[1,2048,512]{2,1,0:T(8,128)(2,1)} %param.31) | copy-start | bytes 6291460
  90.4 25.1 %copy-start.8 = (f32[1,128]{1,0:T(1,128)S(1)}, f32[1,128]{1,0:T(1,128)}, u32[]{:S(2)}) copy-start(f32[1,128]{1,0:T(1,128)} %weight_ref.1) | copy-start | bytes 1540
  90.4 25.1 %copy-start.9 = (f32[1,128]{1,0:T(1,128)S(1)}, f32[1,128]{1,0:T(1,128)}, u32[]{:S(2)}) copy-start(f32[1,128]{1,0:T(1,128)} %share_ref.1) | copy-start | bytes 1540

commit v5 on v4

--- a/solution.py
+++ b/solution.py
@@ -104,11 +104,11 @@
     scale = float(HEAD_DIM ** (-0.5) * np.log2(np.e))
 
     def score(i, score_ref):
-        rows = pl.ds(pl.multiple_of(i * block, block), block)
+        rows = pl.ds(i * block, block)
         score_ref[...] = dot(x_ref[rows, 0:HEAD_DIM], x_ref[:, HEAD_DIM : 2 * HEAD_DIM], ((1,), (1,)))
 
     def mix(i, score_ref):
-        rows = pl.ds(pl.multiple_of(i * block, block), block)
+        rows = pl.ds(i * block, block)
         top = jnp.max(score_ref[...], axis=-1, keepdims=True)
         weights = jnp.exp2((score_ref[...] - top) * scale).astype(BF16)
         both = dot(weights, value_ref[...])
@@ -116,15 +116,11 @@
 
     score(0, even_ref)
 
-    def two(j, carry):
-        i = 2 * j
-        score(i + 1, odd_ref)
-        mix(i, even_ref)
-        score(jnp.minimum(i + 2, blocks - 1), even_ref)
-        mix(i + 1, odd_ref)
-        return carry
-
-    lax.fori_loop(0, blocks // 2, two, 0)
+    refs = (even_ref, odd_ref)
+    for i in range(blocks):
+        if i + 1 < blocks:
+            score(i + 1, refs[(i + 1) % 2])
+        mix(i, refs[i % 2])
 
 
 def rms(floats, gain):
@@ -179,13 +175,15 @@
     blocks = [slice(c * 128, (c + 1) * 128) for c in range(width // 128)]
     for c, cols in enumerate(blocks):
         wide_ref[c] = y_ref[:, cols].astype(F32)
-        for side in range(2):
-            x_ref[side, :, cols] = wide_ref[c, sides[side], :].astype(BF16)
+        x_ref[0, :, cols] = wide_ref[c, sides[0], :].astype(BF16)
     for side in range(2):
         gate_ref, up_ref, down_ref = weights[3 * side : 3 * side + 3]
         if side == 1:
             copies[0].wait()
         gated = dot(x_ref[side], gate_ref[...])
+        if side == 0:
+            for c, cols in enumerate(blocks):
+                x_ref[1, :, cols] = wide_ref[c, sides[1], :].astype(BF16)
         if side == 1:
             copies[1].wait()
         lifted = dot(x_ref[side], up_ref[...])

time: 117 us -> 117 us (level)
  transfers between devices with their start and end apart: 3 -> 3, of which waited for: 0 -> 0; matrix products, arithmetic and copies ran while one was open for 0% -> 0% of each run, Pallas kernels for 15% -> 14%
where the time goes in v5:
time: 117 us; the launch traced here: 116 us
  blocking collectives  89 us (76%)
  Pallas kernels  26.5 us (23%)
    all_to_all x1, blocking collectives, local(): arrived = lax.all_to_all(sent, peers, 0, 0, tiled=True)  26.9 us
    all_to_all x1, blocking collectives, local(): lax.all_to_all(answered.reshape(chips, 2 * CAP, width), peers, 0, 0, tile...  25.1 us
    all_to_all x1, blocking collectives, local(): gathered = lax.all_to_all(packed, line, 0, 0, tiled=True)  23.7 us
    all_to_all x1, blocking collectives, local(): lax.all_to_all(attended.reshape(sp_count, tokens, HEAD_DIM), line, 0, 0,...  13.3 us
    pallas_call x1, Pallas kernels, local(): pl.pallas_call(pack_kernel, grid=(PACK_STEPS,), out_shape=jax.ShapeDtypeS...  11.2 us
    pallas_call x1, Pallas kernels, local(): pl.pallas_call(expert_kernel, out_shape=jax.ShapeDtypeStruct((rows, width...  6.03 us
    pallas_call x1, Pallas kernels, local(): pl.pallas_call(attend_kernel, out_shape=jax.ShapeDtypeStruct((length, HEA...  5.28 us
    pallas_call x1, Pallas kernels, local(): pl.pallas_call(proj_kernel, out_shape=(jax.ShapeDtypeStruct((chips, 2 * C...  2.42 us
  transfers between devices with their start and end apart: 3, of which 0 were waited for; matrix products, arithmetic and copies ran while one was open for 0% of the time, Pallas kernels for 14%

profile of v5, /device:TPU:0, one launch (start us, length us, event | category | flops | bytes accessed | tf_op | source)
XLA Modules:
  0.0 116.2 jit_solution(18078601342431101950)
XLA Ops:
  0.0 0.0 collective-permute-start
  0.0 0.5 collective-permute-start.1
  0.5 0.0 collective-permute-start.2
  0.5 11.2 %pack.1 = bf16[16,128,384]{2,1,0:T(8,128)(2,1)} custom-call(s32[1]{0:T(128)} %bitcast.place_ref, bf16[128,2048]{1,0:T(8,128)(2,1)} %bitcast.36, bf16[128,512]{1,0:T(8,128)(2,1)} %bitcast.37, bf16[128,512]{1,0:T(8,128)(2,1)} %bitcast.38, f32[1,128]{1,0:T(1,128)} %bitcast.39, f32[1,128]{1,0:T(1,128)} %bitcast.40, f32[2,32,128]{2,1,0:T(8,128)} %constant.27.clone.row_ref, ...), custom_call_target="tpu_custom_call" | custom-call | tf_op jit(solution)/shard_map/pack/pallas_call | solution.py:252
  11.7 23.7 %all_to_all.20 = bf16[16,128,384]{2,1,0:T(8,128)(2,1)S(1)} all-to-all(bf16[16,128,384]{2,1,0:T(8,128)(2,1)} %pack.1), channel_id=1, replica_groups=mesh['z'=4,'x'=4,'y'=4,'core'=2] {'x','z'}, dimensions={0} | all-to-all | bytes 3145728 | tf_op jit(solution)/shard_map/all_to_all | solution.py:282
  35.4 0.0 copy-start
  35.4 0.0 copy-start.4
  35.4 0.0 copy-start.5
  35.4 0.0 copy-start.6
  35.4 0.0 copy-start.7
  35.4 5.3 %attend.1 = bf16[2048,128]{1,0:T(8,128)(2,1)S(1)} custom-call(bf16[2048,384]{1,0:T(8,128)(2,1)S(1)} %bitcast.30), custom_call_target="tpu_custom_call" | custom-call | flops 536870912 | bytes 2097152 | tf_op jit(solution)/shard_map/attend/pallas_call | solution.py:284
  40.7 13.3 %all_to_all.21.att_ref = bf16[16,128,128]{2,1,0:T(8,128)(2,1)S(1)} all-to-all(bf16[16,128,128]{2,1,0:T(8,128)(2,1)S(1)} %bitcast.32), channel_id=1, replica_groups=mesh['z'=4,'x'=4,'y'=4,'core'=2] {'x','z'}, dimensions={0} | all-to-all | bytes 1048576 | tf_op jit(solution)/shard_map/all_to_all | solution.py:302
  54.1 0.0 collective-permute-done.rest_0_.rest_3_
  54.1 0.0 collective-permute-done.1.rest_1_.rest_4_
  54.1 0.0 collective-permute-done.2.rest_2_.rest_5_
  54.1 0.0 copy-done
  54.1 0.0 copy-done.4
  54.1 0.0 copy-done.5
  54.1 0.0 copy-done.6
  54.1 0.0 copy-done.7
  54.1 0.0 copy-start.3
  54.2 2.4 %project.1 = (bf16[64,8,2048]{2,1,0:T(8,128)(2,1)S(1)}, bf16[128,2048]{1,0:T(8,128)(2,1)S(1)}, s32[8,128]{1,0:T(8,128)S(1)}) custom-call(s32[1]{0:T(128)} %bitcast.place_ref, bf16[16,128,128]{2,1,0:T(8,128)(2,1)S(1)} %all_to_all.21.att_ref, bf16[2048,2048]{1,0:T(8,128)(2,1)S(1)} %copy-done, bf16[128,2048]{1,0:T(8,128)(2,1)S(1)} %bitcast.31, ...), custom_call_target="tpu_custom_call" | custom-call | tf_op jit(solution)/shard_map/project/pallas_call | solution.py:304
  56.6 0.0 copy-start.1
  56.6 0.0 copy-start.2
  56.6 26.9 %all_to_all.22 = bf16[64,8,2048]{2,1,0:T(8,128)(2,1)S(1)} all-to-all(bf16[64,8,2048]{2,1,0:T(8,128)(2,1)S(1)} %get-tuple-element.8), channel_id=1, replica_groups=mesh['z'=4,'x'=4,'y'=4,'core'=2] {'z','x','y'}, dimensions={0} | all-to-all | bytes 4194304 | tf_op jit(solution)/shard_map/all_to_all | solution.py:329
  83.5 0.0 copy-done.3
  83.5 0.0 copy-done.1
  83.5 0.0 copy-done.2
  83.5 6.0 %expert.1 = bf16[512,2048]{1,0:T(8,128)(2,1)S(1)} custom-call(bf16[512,2048]{1,0:T(8,128)(2,1)S(1)} %bitcast.22, bf16[2048,512]{1,0:T(8,128)(2,1)S(1)} %bitcast.25, bf16[2048,512]{1,0:T(8,128)(2,1)S(1)} %bitcast.27, bf16[512,2048]{1,0:T(8,128)(2,1)S(1)} %bitcast.29, bf16[2048,512]{1,0:T(8,128)(2,1)} %collective-permute-done.rest_0_.rest_3_, ...), custom_call_target="tpu_custom_call" | custom-call | tf_op jit(solution)/shard_map/expert/pallas_call | solution.py:331
  89.5 0.0 copy-start.8
  89.5 0.0 copy-start.9
  89.6 25.1 %all_to_all.23 = bf16[64,8,2048]{2,1,0:T(8,128)(2,1)S(1)} all-to-all(bf16[64,8,2048]{2,1,0:T(8,128)(2,1)S(1)} %bitcast.23), channel_id=1, replica_groups=mesh['z'=4,'x'=4,'y'=4,'core'=2] {'z','x','y'}, dimensions={0} | all-to-all | bytes 4194304 | tf_op jit(solution)/shard_map/all_to_all | solution.py:345
  114.6 0.0 copy-done.8
  114.6 0.0 copy-done.9
  114.6 1.6 %combine.1 = bf16[128,2048]{1,0:T(8,128)(2,1)} custom-call(bf16[512,2048]{1,0:T(8,128)(2,1)S(1)} %bitcast.21, bf16[128,2048]{1,0:T(8,128)(2,1)S(1)} %get-tuple-element.9.stream_ref, s32[8,128]{1,0:T(8,128)S(1)} %get-tuple-element.10.slot_ref, f32[1,128]{1,0:T(1,128)S(1)} %copy-done.8, f32[1,128]{1,0:T(1,128)S(1)} %copy-done.9), custom_call_target="tpu_custom_call" | custom-call | tf_op jit(solution)/shard_map/combine/pallas_call | solution.py:346
Async XLA Ops:
  0.0 54.1 %collective-permute-start = (bf16[2048,512]{1,0:T(8,128)(2,1)}, bf16[2048,512]{1,0:T(8,128)(2,1)}, u32[]{:S(2)}, u32[]{:S(2)}) collective-permute-start(bf16[2048,512]{1,0:T(8,128)(2,1)} %bitcast.24), channel_id=1, source_target_pairs={{0,1},{1,0},{2,3},{3,2},{4,5},{5,4},{6,7},{7,6},{8,9},{9,8},{10,11... | collective-permute-start | bytes 6291464 | tf_op jit(solution)/shard_map/ppermute | solution.py:245
  0.0 54.1 %collective-permute-start.1 = (bf16[2048,512]{1,0:T(8,128)(2,1)}, bf16[2048,512]{1,0:T(8,128)(2,1)}, u32[]{:S(2)}, u32[]{:S(2)}) collective-permute-start(bf16[2048,512]{1,0:T(8,128)(2,1)} %bitcast.26), channel_id=1, source_target_pairs={{0,1},{1,0},{2,3},{3,2},{4,5},{5,4},{6,7},{7,6},{8,9},{9,8},{10,11... | collective-permute-start | bytes 6291464 | tf_op jit(solution)/shard_map/ppermute | solution.py:245
  0.5 53.6 %collective-permute-start.2 = (bf16[512,2048]{1,0:T(8,128)(2,1)}, bf16[512,2048]{1,0:T(8,128)(2,1)}, u32[]{:S(2)}, u32[]{:S(2)}) collective-permute-start(bf16[512,2048]{1,0:T(8,128)(2,1)} %bitcast.28), channel_id=1, source_target_pairs={{0,1},{1,0},{2,3},{3,2},{4,5},{5,4},{6,7},{7,6},{8,9},{9,8},{10,11... | collective-permute-start | bytes 6291464 | tf_op jit(solution)/shard_map/ppermute | solution.py:245
  35.4 18.7 %copy-start = (bf16[2048,2048]{1,0:T(8,128)(2,1)S(1)}, bf16[2048,2048]{1,0:T(8,128)(2,1)}, u32[]{:S(2)}) copy-start(bf16[2048,2048]{1,0:T(8,128)(2,1)} %w_ref.1) | copy-start | bytes 25165828
  35.4 18.7 %copy-start.4 = (bf16[1,128,2048]{2,1,0:T(8,128)(2,1)S(1)}, bf16[1,128,2048]{2,1,0:T(8,128)(2,1)}, u32[]{:S(2)}) copy-start(bf16[1,128,2048]{2,1,0:T(8,128)(2,1)} %param.18) | copy-start | bytes 1572868
  35.4 18.7 %copy-start.5 = (f32[2048]{0:T(1024)S(1)}, f32[2048]{0:T(1024)}, u32[]{:S(2)}) copy-start(f32[2048]{0:T(1024)} %param.25) | copy-start | bytes 24580
  35.4 18.7 %copy-start.6 = (f32[2048]{0:T(1024)S(1)}, f32[2048]{0:T(1024)}, u32[]{:S(2)}) copy-start(f32[2048]{0:T(1024)} %param.26) | copy-start | bytes 24580
  35.4 18.7 %copy-start.7 = (s32[1,128,2]{1,2,0:T(2,128)S(1)}, s32[1,128,2]{1,2,0:T(2,128)}, u32[]{:S(2)}) copy-start(s32[1,128,2]{1,2,0:T(2,128)} %param.27) | copy-start | bytes 3076
  54.1 29.4 %copy-start.3 = (bf16[1,512,2048]{2,1,0:T(8,128)(2,1)S(1)}, bf16[1,512,2048]{2,1,0:T(8,128)(2,1)}, u32[]{:S(2)}) copy-start(bf16[1,512,2048]{2,1,0:T(8,128)(2,1)} %param.32) | copy-start | bytes 6291460
  56.6 26.9 %copy-start.1 = (bf16[1,2048,512]{2,1,0:T(8,128)(2,1)S(1)}, bf16[1,2048,512]{2,1,0:T(8,128)(2,1)}, u32[]{:S(2)}) copy-start(bf16[1,2048,512]{2,1,0:T(8,128)(2,1)} %param.30) | copy-start | bytes 6291460
  56.6 26.9 %copy-start.2 = (bf16[1,2048,512]{2,1,0:T(8,128)(2,1)S(1)}, bf16[1,2048,512]{2,1,0:T(8,128)(2,1)}, u32[]{:S(2)}) copy-start(bf16[1,2048,512]{2,1,0:T(8,128)(2,1)} %param.31) | copy-start | bytes 6291460
  89.5 25.1 %copy-start.8 = (f32[1,128]{1,0:T(1,128)S(1)}, f32[1,128]{1,0:T(1,128)}, u32[]{:S(2)}) copy-start(f32[1,128]{1,0:T(1,128)} %weight_ref.1) | copy-start | bytes 1540
  89.5 25.1 %copy-start.9 = (f32[1,128]{1,0:T(1,128)S(1)}, f32[1,128]{1,0:T(1,128)}, u32[]{:S(2)}) copy-start(f32[1,128]{1,0:T(1,128)} %share_ref.1) | copy-start | bytes 1540

commit v6 on v5

--- a/solution.py
+++ b/solution.py
@@ -127,9 +127,13 @@
     return floats * lax.rsqrt(jnp.mean(floats * floats, axis=-1, keepdims=True) + EPSILON) * gain
 
 
-def proj_kernel(place_ref, att_ref, w_ref, res_ref, post_ref, pre_ref, ids_ref, *rest):
-    *_, out_ref, stream_ref, slot_ref, x_ref = rest
+def proj_kernel(place_ref, att_ref, w_ref, res_ref, post_ref, pre_ref, ids_ref, weight_ref, share_ref, *rest):
+    *_, out_ref, stream_ref, slot_ref, scale_ref, x_ref = rest
     tokens, width = x_ref.shape
+    weight = weight_ref[...]
+    share = share_ref[...]
+    top = lax.broadcasted_iota(jnp.int32, (tokens, tokens), 0) == 0
+    scale_ref[...] = jnp.where(top, weight * share, weight * (1.0 - share)).T
     for h in range(HEADS):
         x_ref[:, h * HEAD_DIM : (h + 1) * HEAD_DIM] = att_ref[h]
     experts = 2 * out_ref.shape[0]
@@ -197,18 +201,13 @@
         out_ref[:, cols] = wide_ref[c].astype(BF16)
 
 
-def combine_kernel(z_ref, stream_ref, slot_ref, weight_ref, share_ref, out_ref):
+def combine_kernel(z_ref, stream_ref, slot_ref, scale_ref, out_ref):
     slots = z_ref.shape[0]
     tokens, width = stream_ref.shape
     slot = lax.broadcasted_iota(jnp.int32, (slots, tokens), 0)
     picks = [jnp.where(slot == slot_ref[i : i + 1, :], 1.0, 0.0).astype(BF16) for i in range(2)]
     picked = dot(jnp.concatenate(picks, axis=1), z_ref[...], ((0,), (0,)))
-    column = lambda row: jnp.broadcast_to(row, (tokens, tokens)).T[:, 0:1]
-    weight = weight_ref[...]
-    share = share_ref[...]
-    weight_first = column(weight * share)
-    weight_second = column(weight * (1.0 - share))
-    ffn = weight_first * picked[0:tokens] + weight_second * picked[tokens:]
+    ffn = scale_ref[:, 0:1] * picked[0:tokens] + scale_ref[:, 1:2] * picked[tokens:]
     out_ref[...] = (stream_ref[...].astype(F32) + ffn).astype(BF16)
 
 
@@ -301,15 +300,16 @@
     )(gathered.reshape(length, 3 * HEAD_DIM))
     attended = lax.all_to_all(attended.reshape(sp_count, tokens, HEAD_DIM), line, 0, 0, tiled=True)
     hbm = pl.BlockSpec(memory_space=pltpu.HBM)
-    sent, stream, slots = pl.pallas_call(
+    sent, stream, slots, scales = pl.pallas_call(
         proj_kernel,
         out_shape=(
             jax.ShapeDtypeStruct((chips, 2 * CAP, width), BF16),
             jax.ShapeDtypeStruct((tokens, width), BF16),
             jax.ShapeDtypeStruct((8, tokens), jnp.int32),
+            jax.ShapeDtypeStruct((tokens, tokens), F32),
         ),
-        in_specs=[smem] + [vmem] * 6 + [hbm] * 3,
-        out_specs=(vmem,) * 3,
+        in_specs=[smem] + [vmem] * 8 + [hbm] * 3,
+        out_specs=(vmem,) * 4,
         scratch_shapes=[
             pltpu.VMEM((tokens, width), BF16),
         ],
@@ -323,6 +323,8 @@
         post_gain[None],
         pre_gain[None],
         route_ids[0].T,
+        group_weight,
+        first_share,
         *partner,
     )
     peers = ("z", "x", "y")
@@ -346,11 +348,11 @@
     combined = pl.pallas_call(
         combine_kernel,
         out_shape=jax.ShapeDtypeStruct((tokens, width), BF16),
-        in_specs=[vmem] * 5,
+        in_specs=[vmem] * 4,
         out_specs=vmem,
         compiler_params=limit(16),
         name="combine",
-    )(returned.reshape(rows, width), stream, slots, group_weight, first_share)
+    )(returned.reshape(rows, width), stream, slots, scales)
     return combined[None]
 
 

time: 117 us -> 116 us (level)
  no operation moved by 1% of the time
where the time goes in v6:
time: 116 us
  blocking collectives  89 us (77%)
  Pallas kernels  26.4 us (23%)
    all_to_all x1, blocking collectives, local(): arrived = lax.all_to_all(sent, peers, 0, 0, tiled=True)  26.9 us
    all_to_all x1, blocking collectives, local(): lax.all_to_all(answered.reshape(chips, 2 * CAP, width), peers, 0, 0, tile...  25.1 us
    all_to_all x1, blocking collectives, local(): gathered = lax.all_to_all(packed, line, 0, 0, tiled=True)  23.7 us
    all_to_all x1, blocking collectives, local(): lax.all_to_all(attended.reshape(sp_count, tokens, HEAD_DIM), line, 0, 0,...  13.3 us
    pallas_call x1, Pallas kernels, local(): pl.pallas_call(pack_kernel, grid=(PACK_STEPS,), out_shape=jax.ShapeDtypeS...  11.2 us
    pallas_call x1, Pallas kernels, local(): pl.pallas_call(expert_kernel, out_shape=jax.ShapeDtypeStruct((rows, width...  6.03 us
    pallas_call x1, Pallas kernels, local(): pl.pallas_call(attend_kernel, out_shape=jax.ShapeDtypeStruct((length, HEA...  5.13 us
    pallas_call x1, Pallas kernels, local(): pl.pallas_call(proj_kernel, out_shape=(jax.ShapeDtypeStruct((chips, 2 * C...  2.46 us
  transfers between devices with their start and end apart: 3, of which 0 were waited for; matrix products, arithmetic and copies ran while one was open for 0% of the time, Pallas kernels for 14%

profile of v6, /device:TPU:0, one launch (start us, length us, event | category | flops | bytes accessed | tf_op | source)
XLA Modules:
  0.0 116.1 jit_solution(1496105676374190420)
XLA Ops:
  0.0 0.0 collective-permute-start
  0.0 0.5 collective-permute-start.1
  0.5 0.0 collective-permute-start.2
  0.5 11.2 %pack.1 = bf16[16,128,384]{2,1,0:T(8,128)(2,1)} custom-call(s32[1]{0:T(128)} %bitcast.place_ref, bf16[128,2048]{1,0:T(8,128)(2,1)} %bitcast.36, bf16[128,512]{1,0:T(8,128)(2,1)} %bitcast.37, bf16[128,512]{1,0:T(8,128)(2,1)} %bitcast.38, f32[1,128]{1,0:T(1,128)} %bitcast.39, f32[1,128]{1,0:T(1,128)} %bitcast.40, f32[2,32,128]{2,1,0:T(8,128)} %constant.27.clone.row_ref, ...), custom_call_target="tpu_custom_call" | custom-call | tf_op jit(solution)/shard_map/pack/pallas_call | solution.py:251
  11.7 23.7 %all_to_all.20 = bf16[16,128,384]{2,1,0:T(8,128)(2,1)S(1)} all-to-all(bf16[16,128,384]{2,1,0:T(8,128)(2,1)} %pack.1), channel_id=1, replica_groups=mesh['z'=4,'x'=4,'y'=4,'core'=2] {'x','z'}, dimensions={0} | all-to-all | bytes 3145728 | tf_op jit(solution)/shard_map/all_to_all | solution.py:281
  35.4 0.0 copy-start
  35.4 0.0 copy-start.4
  35.4 0.0 copy-start.5
  35.4 0.0 copy-start.6
  35.4 0.0 copy-start.7
  35.4 0.0 copy-start.8
  35.5 0.0 copy-start.9
  35.5 5.1 %attend.1 = bf16[2048,128]{1,0:T(8,128)(2,1)S(1)} custom-call(bf16[2048,384]{1,0:T(8,128)(2,1)S(1)} %bitcast.30), custom_call_target="tpu_custom_call" | custom-call | flops 536870912 | bytes 2097152 | tf_op jit(solution)/shard_map/attend/pallas_call | solution.py:283
  40.6 13.3 %all_to_all.21.att_ref = bf16[16,128,128]{2,1,0:T(8,128)(2,1)S(1)} all-to-all(bf16[16,128,128]{2,1,0:T(8,128)(2,1)S(1)} %bitcast.32), channel_id=1, replica_groups=mesh['z'=4,'x'=4,'y'=4,'core'=2] {'x','z'}, dimensions={0} | all-to-all | bytes 1048576 | tf_op jit(solution)/shard_map/all_to_all | solution.py:301
  54.0 0.0 collective-permute-done.rest_0_.rest_3_
  54.0 0.0 collective-permute-done.1.rest_1_.rest_4_
  54.0 0.0 collective-permute-done.2.rest_2_.rest_5_
  54.0 0.0 copy-done
  54.0 0.0 copy-done.4
  54.0 0.0 copy-done.5
  54.0 0.0 copy-done.6
  54.0 0.0 copy-done.7
  54.0 0.0 copy-done.8
  54.0 0.0 copy-done.9
  54.0 0.0 copy-start.3
  54.0 2.5 %project.1 = (bf16[64,8,2048]{2,1,0:T(8,128)(2,1)S(1)}, bf16[128,2048]{1,0:T(8,128)(2,1)S(1)}, s32[8,128]{1,0:T(8,128)S(1)}, f32[128,128]{1,0:T(8,128)S(1)}) custom-call(s32[1]{0:T(128)} %bitcast.place_ref, bf16[16,128,128]{2,1,0:T(8,128)(2,1)S(1)} %all_to_all.21.att_ref, bf16[2048,2048]{1,0:T(8,128)(2,1)S(1)} %copy-done, bf16[128,2048]{1,0:T(8,128)(2,1)S(1)} %bitcast.31, ...), custom_call_target="tpu_custom_call" | custom-call | tf_op jit(solution)/shard_map/project/pallas_call | solution.py:303
  56.5 0.0 copy-start.1
  56.5 0.0 copy-start.2
  56.5 26.9 %all_to_all.22 = bf16[64,8,2048]{2,1,0:T(8,128)(2,1)S(1)} all-to-all(bf16[64,8,2048]{2,1,0:T(8,128)(2,1)S(1)} %get-tuple-element.9), channel_id=1, replica_groups=mesh['z'=4,'x'=4,'y'=4,'core'=2] {'z','x','y'}, dimensions={0} | all-to-all | bytes 4194304 | tf_op jit(solution)/shard_map/all_to_all | solution.py:331
  83.4 0.0 copy-done.3
  83.4 0.0 copy-done.1
  83.4 0.0 copy-done.2
  83.4 6.0 %expert.1 = bf16[512,2048]{1,0:T(8,128)(2,1)S(1)} custom-call(bf16[512,2048]{1,0:T(8,128)(2,1)S(1)} %bitcast.22, bf16[2048,512]{1,0:T(8,128)(2,1)S(1)} %bitcast.25, bf16[2048,512]{1,0:T(8,128)(2,1)S(1)} %bitcast.27, bf16[512,2048]{1,0:T(8,128)(2,1)S(1)} %bitcast.29, bf16[2048,512]{1,0:T(8,128)(2,1)} %collective-permute-done.rest_0_.rest_3_, ...), custom_call_target="tpu_custom_call" | custom-call | tf_op jit(solution)/shard_map/expert/pallas_call | solution.py:333
  89.5 25.1 %all_to_all.23 = bf16[64,8,2048]{2,1,0:T(8,128)(2,1)S(1)} all-to-all(bf16[64,8,2048]{2,1,0:T(8,128)(2,1)S(1)} %bitcast.23), channel_id=1, replica_groups=mesh['z'=4,'x'=4,'y'=4,'core'=2] {'z','x','y'}, dimensions={0} | all-to-all | bytes 4194304 | tf_op jit(solution)/shard_map/all_to_all | solution.py:347
  114.5 1.6 %combine.1 = bf16[128,2048]{1,0:T(8,128)(2,1)} custom-call(bf16[512,2048]{1,0:T(8,128)(2,1)S(1)} %bitcast.21, bf16[128,2048]{1,0:T(8,128)(2,1)S(1)} %get-tuple-element.10.stream_ref, s32[8,128]{1,0:T(8,128)S(1)} %get-tuple-element.11.slot_ref, f32[128,128]{1,0:T(8,128)S(1)} %get-tuple-element.12.scale_ref), custom_call_target="tpu_custom_call" | custom-call | tf_op jit(solution)/shard_map/combine/pallas_call | solution.py:348
Async XLA Ops:
  0.0 54.0 %collective-permute-start = (bf16[2048,512]{1,0:T(8,128)(2,1)}, bf16[2048,512]{1,0:T(8,128)(2,1)}, u32[]{:S(2)}, u32[]{:S(2)}) collective-permute-start(bf16[2048,512]{1,0:T(8,128)(2,1)} %bitcast.24), channel_id=1, source_target_pairs={{0,1},{1,0},{2,3},{3,2},{4,5},{5,4},{6,7},{7,6},{8,9},{9,8},{10,11... | collective-permute-start | bytes 6291464 | tf_op jit(solution)/shard_map/ppermute | solution.py:244
  0.0 54.0 %collective-permute-start.1 = (bf16[2048,512]{1,0:T(8,128)(2,1)}, bf16[2048,512]{1,0:T(8,128)(2,1)}, u32[]{:S(2)}, u32[]{:S(2)}) collective-permute-start(bf16[2048,512]{1,0:T(8,128)(2,1)} %bitcast.26), channel_id=1, source_target_pairs={{0,1},{1,0},{2,3},{3,2},{4,5},{5,4},{6,7},{7,6},{8,9},{9,8},{10,11... | collective-permute-start | bytes 6291464 | tf_op jit(solution)/shard_map/ppermute | solution.py:244
  0.5 53.4 %collective-permute-start.2 = (bf16[512,2048]{1,0:T(8,128)(2,1)}, bf16[512,2048]{1,0:T(8,128)(2,1)}, u32[]{:S(2)}, u32[]{:S(2)}) collective-permute-start(bf16[512,2048]{1,0:T(8,128)(2,1)} %bitcast.28), channel_id=1, source_target_pairs={{0,1},{1,0},{2,3},{3,2},{4,5},{5,4},{6,7},{7,6},{8,9},{9,8},{10,11... | collective-permute-start | bytes 6291464 | tf_op jit(solution)/shard_map/ppermute | solution.py:244
  35.4 18.5 %copy-start = (bf16[2048,2048]{1,0:T(8,128)(2,1)S(1)}, bf16[2048,2048]{1,0:T(8,128)(2,1)}, u32[]{:S(2)}) copy-start(bf16[2048,2048]{1,0:T(8,128)(2,1)} %w_ref.1) | copy-start | bytes 25165828
  35.4 18.6 %copy-start.4 = (bf16[1,128,2048]{2,1,0:T(8,128)(2,1)S(1)}, bf16[1,128,2048]{2,1,0:T(8,128)(2,1)}, u32[]{:S(2)}) copy-start(bf16[1,128,2048]{2,1,0:T(8,128)(2,1)} %param.18) | copy-start | bytes 1572868
  35.4 18.6 %copy-start.5 = (f32[2048]{0:T(1024)S(1)}, f32[2048]{0:T(1024)}, u32[]{:S(2)}) copy-start(f32[2048]{0:T(1024)} %param.25) | copy-start | bytes 24580
  35.4 18.6 %copy-start.6 = (f32[2048]{0:T(1024)S(1)}, f32[2048]{0:T(1024)}, u32[]{:S(2)}) copy-start(f32[2048]{0:T(1024)} %param.26) | copy-start | bytes 24580
  35.4 18.6 %copy-start.7 = (s32[1,128,2]{1,2,0:T(2,128)S(1)}, s32[1,128,2]{1,2,0:T(2,128)}, u32[]{:S(2)}) copy-start(s32[1,128,2]{1,2,0:T(2,128)} %param.27) | copy-start | bytes 3076
  35.4 18.6 %copy-start.8 = (f32[1,128]{1,0:T(1,128)S(1)}, f32[1,128]{1,0:T(1,128)}, u32[]{:S(2)}) copy-start(f32[1,128]{1,0:T(1,128)} %weight_ref.1) | copy-start | bytes 1540
  35.5 18.6 %copy-start.9 = (f32[1,128]{1,0:T(1,128)S(1)}, f32[1,128]{1,0:T(1,128)}, u32[]{:S(2)}) copy-start(f32[1,128]{1,0:T(1,128)} %share_ref.1) | copy-start | bytes 1540
  54.0 29.4 %copy-start.3 = (bf16[1,512,2048]{2,1,0:T(8,128)(2,1)S(1)}, bf16[1,512,2048]{2,1,0:T(8,128)(2,1)}, u32[]{:S(2)}) copy-start(bf16[1,512,2048]{2,1,0:T(8,128)(2,1)} %param.32) | copy-start | bytes 6291460
  56.5 26.9 %copy-start.1 = (bf16[1,2048,512]{2,1,0:T(8,128)(2,1)S(1)}, bf16[1,2048,512]{2,1,0:T(8,128)(2,1)}, u32[]{:S(2)}) copy-start(bf16[1,2048,512]{2,1,0:T(8,128)(2,1)} %param.30) | copy-start | bytes 6291460
  56.5 26.9 %copy-start.2 = (bf16[1,2048,512]{2,1,0:T(8,128)(2,1)S(1)}, bf16[1,2048,512]{2,1,0:T(8,128)(2,1)}, u32[]{:S(2)}) copy-start(bf16[1,2048,512]{2,1,0:T(8,128)(2,1)} %param.31) | copy-start | bytes 6291460

commit v7 on v5

--- a/solution.py
+++ b/solution.py
@@ -16,7 +16,7 @@
 CAP = 4
 EPSILON = 1e-06
 LATE_CORE = 0
-PACK_STEPS = 2
+PACK_STEPS = 1
 STAGGER_NS = 8200
 F32 = jnp.float32
 BF16 = jnp.bfloat16

time: 117 us -> 117 us (level)
  no operation moved by 1% of the time
where the time goes in v7:
time: 117 us; the launch traced here: 116 us
  blocking collectives  89 us (76%)
  Pallas kernels  26.7 us (23%)
    all_to_all x1, blocking collectives, local(): arrived = lax.all_to_all(sent, peers, 0, 0, tiled=True)  26.9 us
    all_to_all x1, blocking collectives, local(): lax.all_to_all(answered.reshape(chips, 2 * CAP, width), peers, 0, 0, tile...  25.1 us
    all_to_all x1, blocking collectives, local(): gathered = lax.all_to_all(packed, line, 0, 0, tiled=True)  23.7 us
    all_to_all x1, blocking collectives, local(): lax.all_to_all(attended.reshape(sp_count, tokens, HEAD_DIM), line, 0, 0,...  13.3 us
    pallas_call x1, Pallas kernels, local(): pl.pallas_call(pack_kernel, grid=(PACK_STEPS,), out_shape=jax.ShapeDtypeS...  11.4 us
    pallas_call x1, Pallas kernels, local(): pl.pallas_call(expert_kernel, out_shape=jax.ShapeDtypeStruct((rows, width...  6.02 us
    pallas_call x1, Pallas kernels, local(): pl.pallas_call(attend_kernel, out_shape=jax.ShapeDtypeStruct((length, HEA...  5.28 us
    pallas_call x1, Pallas kernels, local(): pl.pallas_call(proj_kernel, out_shape=(jax.ShapeDtypeStruct((chips, 2 * C...  2.42 us
  transfers between devices with their start and end apart: 3, of which 0 were waited for; matrix products, arithmetic and copies ran while one was open for 0% of the time, Pallas kernels for 14%

profile of v7, /device:TPU:0, one launch (start us, length us, event | category | flops | bytes accessed | tf_op | source)
XLA Modules:
  0.0 116.4 jit_solution(6368902546117297485)
XLA Ops:
  0.0 0.0 collective-permute-start
  0.0 0.5 collective-permute-start.1
  0.5 0.0 collective-permute-start.2
  0.5 11.4 %pack.1 = bf16[16,128,384]{2,1,0:T(8,128)(2,1)} custom-call(s32[1]{0:T(128)} %bitcast.place_ref, bf16[128,2048]{1,0:T(8,128)(2,1)} %bitcast.36, bf16[128,512]{1,0:T(8,128)(2,1)} %bitcast.37, bf16[128,512]{1,0:T(8,128)(2,1)} %bitcast.38, f32[1,128]{1,0:T(1,128)} %bitcast.39, f32[1,128]{1,0:T(1,128)} %bitcast.40, f32[2,32,128]{2,1,0:T(8,128)} %constant.27.clone.row_ref, ...), custom_call_target="tpu_custom_call" | custom-call | tf_op jit(solution)/shard_map/pack/pallas_call | solution.py:252
  11.9 23.7 %all_to_all.20 = bf16[16,128,384]{2,1,0:T(8,128)(2,1)S(1)} all-to-all(bf16[16,128,384]{2,1,0:T(8,128)(2,1)} %pack.1), channel_id=1, replica_groups=mesh['z'=4,'x'=4,'y'=4,'core'=2] {'x','z'}, dimensions={0} | all-to-all | bytes 3145728 | tf_op jit(solution)/shard_map/all_to_all | solution.py:282
  35.6 0.0 copy-start
  35.6 0.0 copy-start.4
  35.6 0.0 copy-start.5
  35.6 0.0 copy-start.6
  35.6 0.0 copy-start.7
  35.6 5.3 %attend.1 = bf16[2048,128]{1,0:T(8,128)(2,1)S(1)} custom-call(bf16[2048,384]{1,0:T(8,128)(2,1)S(1)} %bitcast.30), custom_call_target="tpu_custom_call" | custom-call | flops 536870912 | bytes 2097152 | tf_op jit(solution)/shard_map/attend/pallas_call | solution.py:284
  40.9 13.3 %all_to_all.21.att_ref = bf16[16,128,128]{2,1,0:T(8,128)(2,1)S(1)} all-to-all(bf16[16,128,128]{2,1,0:T(8,128)(2,1)S(1)} %bitcast.32), channel_id=1, replica_groups=mesh['z'=4,'x'=4,'y'=4,'core'=2] {'x','z'}, dimensions={0} | all-to-all | bytes 1048576 | tf_op jit(solution)/shard_map/all_to_all | solution.py:302
  54.2 0.0 collective-permute-done.rest_0_.rest_3_
  54.2 0.0 collective-permute-done.1.rest_1_.rest_4_
  54.2 0.0 collective-permute-done.2.rest_2_.rest_5_
  54.2 0.0 copy-done
  54.3 0.0 copy-done.4
  54.3 0.0 copy-done.5
  54.3 0.0 copy-done.6
  54.3 0.0 copy-done.7
  54.3 0.0 copy-start.3
  54.3 2.4 %project.1 = (bf16[64,8,2048]{2,1,0:T(8,128)(2,1)S(1)}, bf16[128,2048]{1,0:T(8,128)(2,1)S(1)}, s32[8,128]{1,0:T(8,128)S(1)}) custom-call(s32[1]{0:T(128)} %bitcast.place_ref, bf16[16,128,128]{2,1,0:T(8,128)(2,1)S(1)} %all_to_all.21.att_ref, bf16[2048,2048]{1,0:T(8,128)(2,1)S(1)} %copy-done, bf16[128,2048]{1,0:T(8,128)(2,1)S(1)} %bitcast.31, ...), custom_call_target="tpu_custom_call" | custom-call | tf_op jit(solution)/shard_map/project/pallas_call | solution.py:304
  56.7 0.0 copy-start.1
  56.7 0.0 copy-start.2
  56.8 26.9 %all_to_all.22 = bf16[64,8,2048]{2,1,0:T(8,128)(2,1)S(1)} all-to-all(bf16[64,8,2048]{2,1,0:T(8,128)(2,1)S(1)} %get-tuple-element.8), channel_id=1, replica_groups=mesh['z'=4,'x'=4,'y'=4,'core'=2] {'z','x','y'}, dimensions={0} | all-to-all | bytes 4194304 | tf_op jit(solution)/shard_map/all_to_all | solution.py:329
  83.6 0.0 copy-done.3
  83.6 0.0 copy-done.1
  83.7 0.0 copy-done.2
  83.7 6.0 %expert.1 = bf16[512,2048]{1,0:T(8,128)(2,1)S(1)} custom-call(bf16[512,2048]{1,0:T(8,128)(2,1)S(1)} %bitcast.22, bf16[2048,512]{1,0:T(8,128)(2,1)S(1)} %bitcast.25, bf16[2048,512]{1,0:T(8,128)(2,1)S(1)} %bitcast.27, bf16[512,2048]{1,0:T(8,128)(2,1)S(1)} %bitcast.29, bf16[2048,512]{1,0:T(8,128)(2,1)} %collective-permute-done.rest_0_.rest_3_, ...), custom_call_target="tpu_custom_call" | custom-call | tf_op jit(solution)/shard_map/expert/pallas_call | solution.py:331
  89.7 0.0 copy-start.8
  89.7 0.0 copy-start.9
  89.7 25.1 %all_to_all.23 = bf16[64,8,2048]{2,1,0:T(8,128)(2,1)S(1)} all-to-all(bf16[64,8,2048]{2,1,0:T(8,128)(2,1)S(1)} %bitcast.23), channel_id=1, replica_groups=mesh['z'=4,'x'=4,'y'=4,'core'=2] {'z','x','y'}, dimensions={0} | all-to-all | bytes 4194304 | tf_op jit(solution)/shard_map/all_to_all | solution.py:345
  114.8 0.0 copy-done.8
  114.8 0.0 copy-done.9
  114.8 1.6 %combine.1 = bf16[128,2048]{1,0:T(8,128)(2,1)} custom-call(bf16[512,2048]{1,0:T(8,128)(2,1)S(1)} %bitcast.21, bf16[128,2048]{1,0:T(8,128)(2,1)S(1)} %get-tuple-element.9.stream_ref, s32[8,128]{1,0:T(8,128)S(1)} %get-tuple-element.10.slot_ref, f32[1,128]{1,0:T(1,128)S(1)} %copy-done.8, f32[1,128]{1,0:T(1,128)S(1)} %copy-done.9), custom_call_target="tpu_custom_call" | custom-call | tf_op jit(solution)/shard_map/combine/pallas_call | solution.py:346
Async XLA Ops:
  0.0 54.2 %collective-permute-start = (bf16[2048,512]{1,0:T(8,128)(2,1)}, bf16[2048,512]{1,0:T(8,128)(2,1)}, u32[]{:S(2)}, u32[]{:S(2)}) collective-permute-start(bf16[2048,512]{1,0:T(8,128)(2,1)} %bitcast.24), channel_id=1, source_target_pairs={{0,1},{1,0},{2,3},{3,2},{4,5},{5,4},{6,7},{7,6},{8,9},{9,8},{10,11... | collective-permute-start | bytes 6291464 | tf_op jit(solution)/shard_map/ppermute | solution.py:245
  0.0 54.2 %collective-permute-start.1 = (bf16[2048,512]{1,0:T(8,128)(2,1)}, bf16[2048,512]{1,0:T(8,128)(2,1)}, u32[]{:S(2)}, u32[]{:S(2)}) collective-permute-start(bf16[2048,512]{1,0:T(8,128)(2,1)} %bitcast.26), channel_id=1, source_target_pairs={{0,1},{1,0},{2,3},{3,2},{4,5},{5,4},{6,7},{7,6},{8,9},{9,8},{10,11... | collective-permute-start | bytes 6291464 | tf_op jit(solution)/shard_map/ppermute | solution.py:245
  0.5 53.7 %collective-permute-start.2 = (bf16[512,2048]{1,0:T(8,128)(2,1)}, bf16[512,2048]{1,0:T(8,128)(2,1)}, u32[]{:S(2)}, u32[]{:S(2)}) collective-permute-start(bf16[512,2048]{1,0:T(8,128)(2,1)} %bitcast.28), channel_id=1, source_target_pairs={{0,1},{1,0},{2,3},{3,2},{4,5},{5,4},{6,7},{7,6},{8,9},{9,8},{10,11... | collective-permute-start | bytes 6291464 | tf_op jit(solution)/shard_map/ppermute | solution.py:245
  35.6 18.7 %copy-start = (bf16[2048,2048]{1,0:T(8,128)(2,1)S(1)}, bf16[2048,2048]{1,0:T(8,128)(2,1)}, u32[]{:S(2)}) copy-start(bf16[2048,2048]{1,0:T(8,128)(2,1)} %w_ref.1) | copy-start | bytes 25165828
  35.6 18.7 %copy-start.4 = (bf16[1,128,2048]{2,1,0:T(8,128)(2,1)S(1)}, bf16[1,128,2048]{2,1,0:T(8,128)(2,1)}, u32[]{:S(2)}) copy-start(bf16[1,128,2048]{2,1,0:T(8,128)(2,1)} %param.18) | copy-start | bytes 1572868
  35.6 18.7 %copy-start.5 = (f32[2048]{0:T(1024)S(1)}, f32[2048]{0:T(1024)}, u32[]{:S(2)}) copy-start(f32[2048]{0:T(1024)} %param.25) | copy-start | bytes 24580
  35.6 18.7 %copy-start.6 = (f32[2048]{0:T(1024)S(1)}, f32[2048]{0:T(1024)}, u32[]{:S(2)}) copy-start(f32[2048]{0:T(1024)} %param.26) | copy-start | bytes 24580
  35.6 18.7 %copy-start.7 = (s32[1,128,2]{1,2,0:T(2,128)S(1)}, s32[1,128,2]{1,2,0:T(2,128)}, u32[]{:S(2)}) copy-start(s32[1,128,2]{1,2,0:T(2,128)} %param.27) | copy-start | bytes 3076
  54.3 29.4 %copy-start.3 = (bf16[1,512,2048]{2,1,0:T(8,128)(2,1)S(1)}, bf16[1,512,2048]{2,1,0:T(8,128)(2,1)}, u32[]{:S(2)}) copy-start(bf16[1,512,2048]{2,1,0:T(8,128)(2,1)} %param.32) | copy-start | bytes 6291460
  56.7 26.9 %copy-start.1 = (bf16[1,2048,512]{2,1,0:T(8,128)(2,1)S(1)}, bf16[1,2048,512]{2,1,0:T(8,128)(2,1)}, u32[]{:S(2)}) copy-start(bf16[1,2048,512]{2,1,0:T(8,128)(2,1)} %param.30) | copy-start | bytes 6291460
  56.7 26.9 %copy-start.2 = (bf16[1,2048,512]{2,1,0:T(8,128)(2,1)S(1)}, bf16[1,2048,512]{2,1,0:T(8,128)(2,1)}, u32[]{:S(2)}) copy-start(bf16[1,2048,512]{2,1,0:T(8,128)(2,1)} %param.31) | copy-start | bytes 6291460
  89.7 25.1 %copy-start.8 = (f32[1,128]{1,0:T(1,128)S(1)}, f32[1,128]{1,0:T(1,128)}, u32[]{:S(2)}) copy-start(f32[1,128]{1,0:T(1,128)} %weight_ref.1) | copy-start | bytes 1540
  89.7 25.1 %copy-start.9 = (f32[1,128]{1,0:T(1,128)S(1)}, f32[1,128]{1,0:T(1,128)}, u32[]{:S(2)}) copy-start(f32[1,128]{1,0:T(1,128)} %share_ref.1) | copy-start | bytes 1540
